TPU v7x, 32 devices: a whole 2x2x4 slice. The times are simulated.
32 devices in a mesh: kv: 8 (over z, y), tp: 4 (over x, core).
Axes of the slice: x: 2, y: 2, z: 4, core: 2. Of those that a mesh axis runs over, the one named last changes fastest.
Arguments:
- queries: bfloat16 [6144, 2048], P('kv', 'tp'), may hold values from -6 to 6
- keys_values: bfloat16 [6144, 1024], P('kv', 'tp'), may hold values from -6 to 6
- log_sums: float32 [6144, 32], P('kv', 'tp'), may hold values from 6.5 to 7.5
- out_grad: bfloat16 [6144, 2048], P('kv', 'tp'), may hold values from -96 to 96
- inputs: bfloat16 [6144, 4096], P('kv'), may hold values from -0.046875 to 0.046875
- chosen: int32 [48, 16], P('kv'), may hold values from -1 to 95, as said below
Outputs:
- query_grad: bfloat16 [6144, 2048], P('kv', 'tp')
- kv_grad: float32 [6144, 1024], P('kv', 'tp')
- weight_grad: float32 [4096, 2048], P('kv', 'tp')
Inputs may be any that keep to these rules, and one draw needn't show every extreme that they name: `chosen`: each row names distinct key blocks, none starting after the last position of that row's query block, and -1 in unused entries; at least half of 16 blocks are named where that many are allowed. From the query blocks of one index of kv, at most 6 distinct blocks of the 768 positions of any one index are named, and this most is reached on every index.
All inputs are finite; a program needn't handle non-finite values.
Results may differ from a plain program's by a relative error of at most 0.0051.
Values may be sent and summed in bfloat16 or wider, within the bound.
No kernel may reach another device: no remote copies, remote signals or barrier semaphores. Data moves between devices by JAX's collectives and lax.ppermute only.
A program may use at most 128 MiB of HBM per device.

v0:
```python
import jax
import jax.numpy as jnp
from jax import lax
from jax.sharding import PartitionSpec as P

DH = 64
BLK = 64
QB = 128
NSEL = 16


def shards(queries, keys_values, log_sums, out_grad, inputs, chosen):
    score_scale = DH ** (-0.5)
    tok_count = queries.shape[0]
    heads_here = queries.shape[1] // DH
    kv_heads = keys_values.shape[1] // (2 * DH)
    group_size = heads_here // kv_heads
    row_width = keys_values.shape[1]
    blocks_here = tok_count // BLK
    query_blocks = tok_count // QB
    kv_count = lax.axis_size("kv")
    first_block = lax.axis_index("kv") * query_blocks
    capacity = blocks_here // 2
    total_blocks = kv_count * blocks_here
    flat_ids = chosen.reshape(-1)
    needed = jnp.any(
        flat_ids[:, None] == jnp.arange(total_blocks, dtype=jnp.int32)[None, :], axis=0
    )
    needed = needed.reshape(kv_count, blocks_here).astype(jnp.int32)
    rank_in = jnp.cumsum(needed, axis=1) - 1
    matches = (needed[:, :, None] == 1) & (
        rank_in[:, :, None] == jnp.arange(capacity, dtype=jnp.int32)[None, None, :]
    )
    request = jnp.sum(
        matches.astype(jnp.int32) * jnp.arange(blocks_here, dtype=jnp.int32)[None, :, None], axis=1
    )
    request = jnp.where(jnp.any(matches, axis=1), request, -1)
    slot_flat = (jnp.arange(kv_count, dtype=jnp.int32)[:, None] * capacity + rank_in).reshape(-1)
    slot_ids = jnp.where(chosen >= 0, slot_flat[jnp.maximum(chosen, 0)], 0)
    asked_ids = lax.all_to_all(request, "kv", split_axis=0, concat_axis=0, tiled=True)
    local_blocks = keys_values.reshape(blocks_here, BLK, row_width)
    fetched = local_blocks[jnp.maximum(asked_ids, 0)]
    key_table = lax.all_to_all(fetched, "kv", split_axis=0, concat_axis=0, tiled=True).reshape(
        kv_count * capacity, BLK, row_width
    )

    def one_block(grad_table, packed):
        query_rows, grad_rows, sum_rows, chosen_row, slot_row, offset = packed
        query_blk = query_rows.reshape(QB, kv_heads, group_size, DH)
        grad_blk = grad_rows.reshape(QB, kv_heads, group_size, DH)
        sums_blk = sum_rows.reshape(QB, kv_heads, group_size)
        picked = key_table[slot_row].reshape(NSEL * BLK, kv_heads, 2, DH)
        key_blk = picked[:, :, 0, :]
        value_blk = picked[:, :, 1, :]
        present = chosen_row >= 0
        key_pos = (
            jnp.maximum(chosen_row, 0)[:, None] * BLK + jnp.arange(BLK, dtype=jnp.int32)[None, :]
        ).reshape(-1)
        key_live = jnp.repeat(present, BLK)
        query_pos = (first_block + offset) * QB + jnp.arange(QB, dtype=jnp.int32)
        visible = key_live[None, :] & (key_pos[None, :] <= query_pos[:, None])
        scores = (
            jnp.einsum("qhgd,nhd->qhgn", query_blk, key_blk, preferred_element_type=jnp.float32)
            * score_scale
        )
        attn_prob = jnp.where(
            visible[:, None, None, :], jnp.exp(scores - sums_blk[..., None]), jnp.float32(0.0)
        )
        prob_round = attn_prob.astype(jnp.bfloat16)
        output = jnp.einsum(
            "qhgn,nhd->qhgd", prob_round, value_blk, preferred_element_type=jnp.float32
        )
        delta_row = jnp.sum(grad_blk * output, axis=-1)
        prob_grad = jnp.einsum(
            "qhgd,nhd->qhgn", grad_blk, value_blk, preferred_element_type=jnp.float32
        )
        score_round = (attn_prob * (prob_grad - delta_row[..., None])).astype(jnp.bfloat16)
        query_part = (
            score_scale
            * jnp.einsum("qhgn,nhd->qhgd", score_round, key_blk, preferred_element_type=jnp.float32)
        ).astype(jnp.bfloat16)
        key_part = score_scale * jnp.einsum(
            "qhgn,qhgd->nhd", score_round, query_blk, preferred_element_type=jnp.float32
        )
        value_part = jnp.einsum(
            "qhgn,qhgd->nhd", prob_round, grad_blk, preferred_element_type=jnp.float32
        )
        both_parts = jnp.stack([key_part, value_part], axis=2).reshape(NSEL, BLK, row_width)
        return (grad_table.at[slot_row].add(both_parts), query_part.reshape(QB, heads_here * DH))

    packed = (
        queries.reshape(query_blocks, QB, -1),
        out_grad.reshape(query_blocks, QB, -1),
        log_sums.reshape(query_blocks, QB, -1),
        chosen,
        slot_ids,
        jnp.arange(query_blocks, dtype=jnp.int32),
    )
    start_table = jnp.zeros((key_table.shape[0], BLK, row_width), jnp.float32)
    grad_table, query_parts = lax.scan(one_block, start_table, packed)
    query_grad = query_parts.reshape(tok_count, heads_here * DH)
    returned = lax.all_to_all(
        grad_table.reshape(kv_count, capacity, BLK, row_width),
        "kv",
        split_axis=0,
        concat_axis=0,
        tiled=True,
    )
    targets = jnp.where(asked_ids >= 0, asked_ids, blocks_here).reshape(-1)
    summed = (
        jnp.zeros((blocks_here + 1, BLK, row_width), jnp.float32)
        .at[targets]
        .add(returned.reshape(-1, BLK, row_width))
    )
    kv_grad = summed[:blocks_here].reshape(tok_count, row_width)
    weight_grad = lax.psum_scatter(
        lax.dot_general(
            inputs, query_grad, (((0,), (0,)), ((), ())), preferred_element_type=jnp.float32
        ),
        "kv",
        scatter_dimension=0,
        tiled=True,
    )
    return (query_grad, kv_grad, weight_grad)


def solution(mesh):
    in_specs = (
        P("kv", "tp"),
        P("kv", "tp"),
        P("kv", "tp"),
        P("kv", "tp"),
        P("kv", None),
        P("kv", None),
    )
    out_specs = (P("kv", "tp"), P("kv", "tp"), P("kv", "tp"))
    return jax.shard_map(shards, mesh=mesh, in_specs=in_specs, out_specs=out_specs, check_vma=False)
```

profile of v0, /device:TPU:0, one launch (start us, length us, event | category | flops | bytes accessed | tf_op | source)
XLA Modules:
  0.0 514.9 jit_solution(17658362699768816245)
XLA Ops:
  8.9 13.6 %all_to_all.19 = s32[8,1,6]{2,1,0:T(1,128)S(1)} all-to-all(s32[8,1,6]{2,1,0:T(1,128)S(1)} %copy.64), channel_id=1, replica_groups=mesh['kv'=8,'tp'=4] {'kv'}, dimensions={0} | all-to-all | bytes 384 | tf_op jit(solution)/shard_map/all_to_all | solution.py:40
  25.7 4.3 all-to-all-start.1
  31.5 34.4 %all-to-all-done.1 = bf16[8,6,64,256]{3,2,1,0:T(8,128)(2,1)} async-done(((bf16[8,6,64,256]{3,2,1,0:T(8,128)(2,1)}), bf16[8,6,64,256]{3,2,1,0:T(8,128)(2,1)}, u32[]{:S(2)}, u32[]{:S(2)}) %all-to-all-start.1) | async-done | bytes 1572896 | tf_op jit(solution)/shard_map/all_to_all | solution.py:43
  68.6 216.9 %while.12 = (s32[]{:T(128)}, f32[48,64,256]{2,1,0:T(8,128)}, bf16[6,128,512]{2,1,0:T(8,128)(2,1)}, s32[6,16]{1,0:T(8,128)S(1)}, bf16[6,128,512]{2,1,0:T(8,128)(2...) while((s32[]{:T(128)}, f32[48,64,256]{2,1,0:T(8,128)}, ...), condition=%wide.region_7.8_spmd, body=%wide.region_4.7_spmd.sunk | while | flops 821232896 | bytes 62707756 | solution.py:100
  76.4 3.7 fusion.66
  82.7 3.9 convolution_bitcast_fusion.5
  98.8 3.8 scatter_fusion
  112.6 3.7 fusion.66
  118.9 3.9 convolution_bitcast_fusion.5
  135.1 3.8 scatter_fusion
  148.8 3.7 fusion.66
  155.1 3.9 convolution_bitcast_fusion.5
  171.3 3.8 scatter_fusion
  185.1 3.7 fusion.66
  191.4 3.9 convolution_bitcast_fusion.5
  207.5 3.7 scatter_fusion
  221.2 3.7 fusion.66
  227.5 3.9 convolution_bitcast_fusion.5
  257.2 3.7 fusion.66
  263.6 3.9 convolution_bitcast_fusion.5
  285.5 9.7 %convolution_bitcast_fusion.3 = f32[4096,512]{0,1:T(8,128)} fusion(bf16[768,512]{1,0:T(8,128)(2,1)} %bitcast.164, bf16[768,4096]{1,0:T(8,128)(2,1)} %param.12), kind=kOutput, calls=%fused_computation.42 | convolution fusion | flops 3221225472 | bytes 15466496 | tf_op jit(solution)/shard_map/dot_general | solution.py:117
  299.0 136.4 %all-to-all-done.2 = f32[8,6,64,256]{3,2,1,0:T(8,128)S(1)} async-done(((f32[8,6,64,256]{3,2,1,0:T(8,128)}), f32[8,6,64,256]{3,2,1,0:T(8,128)S(1)}, u32[]{:S(2)}, u32[]{:S(2)}) %all-to-all-start.2) | async-done | bytes 3145760 | tf_op jit(solution)/shard_map/all_to_all | solution.py:102
  437.2 6.7 %scatter_fusion.1 = f32[13,64,256]{2,1,0:T(8,128)S(1)} fusion(f32[13,64,256]{2,1,0:T(8,128)S(1)} %broadcast_in_dim.57, s32[48]{0:T(128)S(1)} %fusion.22, f32[48,64,256]{2,1,0:T(8,128)} %bitcast.159), kind=kCustom, calls=%fused_computation.4 | custom fusion | flops 786432 | bytes 9437376 | tf_op jit(solution)/shard_map/scatter-add | solution.py:113
  444.9 60.6 %reduce-scatter.2.cloned.1.call-done = f32[512,512]{0,1:T(8,128)} async-done(((f32[4096,512]{0,1:T(8,128)}), f32[512,512]{0,1:T(8,128)}) %reduce-scatter.2.cloned.1.call-update) | async-done | bytes 1048592 | tf_op jit(solution)/shard_map/reduce_scatter | solution.py:116
  (289 shorter events, 169.6 us)
Async XLA Ops:
  7.2 16.6 %copy-start = (bf16[768,256]{1,0:T(8,128)(2,1)S(1)}, bf16[768,256]{1,0:T(8,128)(2,1)}, u32[]{:S(2)}) copy-start(bf16[768,256]{1,0:T(8,128)(2,1)} %param.9) | copy-start | bytes 1179652
  7.2 22.9 %copy-start.7 = (s32[6,16]{1,0:T(8,128)S(1)}, s32[6,16]{1,0:T(8,128)}, u32[]{:S(2)}) copy-start(s32[6,16]{1,0:T(8,128)} %param.13) | copy-start | bytes 1156
  25.7 40.3 %all-to-all-start.1 = ((bf16[8,6,64,256]{3,2,1,0:T(8,128)(2,1)}), bf16[8,6,64,256]{3,2,1,0:T(8,128)(2,1)}, u32[]{:S(2)}, u32[]{:S(2)}) async-start(bf16[8,6,64,256]{3,2,1,0:T(8,128)(2,1)} %bitcast.32), calls=%async_computation.1 | async-start | bytes 3145728 | tf_op jit(solution)/shard_map/all_to_all | solution.py:43
  30.0 475.6 %reduce-scatter.2.cloned.1.call-start = ((), (), s32[]{:S(2)}) async-start(), calls=%async_computation.4 | async-start | bytes 9437184 | tf_op jit(solution)/shard_map/reduce_scatter | solution.py:116
  75.1 5.7 %copy-start.8 = (s32[6]{0:T(128)S(1)}, s32[6]{0:T(128)}, u32[]{:S(2)}) copy-start(s32[6]{0:T(128)} %get-tuple-element.259) | copy-start | bytes 76 | tf_op jit(solution)/shard_map/while
  75.1 7.6 %copy-start.6 = (bf16[1,128,512]{1,2,0:T(8,128)(2,1)S(1)}, bf16[1,128,512]{1,2,0:T(8,128)(2,1)}, u32[]{:S(2)}) copy-start(bf16[1,128,512]{1,2,0:T(8,128)(2,1)} %copy.96) | copy-start | bytes 393220 | tf_op jit(solution)/shard_map/while
  76.4 10.2 %copy-start.2 = (bf16[1024,2,1,64]{0,3,1,2:T(8,128)(2,1)}, bf16[1024,2,1,64]{0,3,1,2:T(8,128)(2,1)S(1)}, u32[]{:S(2)}) copy-start(bf16[1024,2,1,64]{0,3,1,2:T(8,128)(2,1)S(1)} %copy.98) | copy-start | bytes 786436 | tf_op jit(solution)/shard_map/while
  87.8 3.5 copy-start.1
  111.3 5.7 %copy-start.8 = (s32[6]{0:T(128)S(1)}, s32[6]{0:T(128)}, u32[]{:S(2)}) copy-start(s32[6]{0:T(128)} %get-tuple-element.259) | copy-start | bytes 76 | tf_op jit(solution)/shard_map/while
  111.3 7.6 %copy-start.6 = (bf16[1,128,512]{1,2,0:T(8,128)(2,1)S(1)}, bf16[1,128,512]{1,2,0:T(8,128)(2,1)}, u32[]{:S(2)}) copy-start(bf16[1,128,512]{1,2,0:T(8,128)(2,1)} %copy.96) | copy-start | bytes 393220 | tf_op jit(solution)/shard_map/while
  112.6 10.2 %copy-start.2 = (bf16[1024,2,1,64]{0,3,1,2:T(8,128)(2,1)}, bf16[1024,2,1,64]{0,3,1,2:T(8,128)(2,1)S(1)}, u32[]{:S(2)}) copy-start(bf16[1024,2,1,64]{0,3,1,2:T(8,128)(2,1)S(1)} %copy.98) | copy-start | bytes 786436 | tf_op jit(solution)/shard_map/while
  147.5 5.7 %copy-start.8 = (s32[6]{0:T(128)S(1)}, s32[6]{0:T(128)}, u32[]{:S(2)}) copy-start(s32[6]{0:T(128)} %get-tuple-element.259) | copy-start | bytes 76 | tf_op jit(solution)/shard_map/while
  147.5 7.6 %copy-start.6 = (bf16[1,128,512]{1,2,0:T(8,128)(2,1)S(1)}, bf16[1,128,512]{1,2,0:T(8,128)(2,1)}, u32[]{:S(2)}) copy-start(bf16[1,128,512]{1,2,0:T(8,128)(2,1)} %copy.96) | copy-start | bytes 393220 | tf_op jit(solution)/shard_map/while
  148.8 10.2 %copy-start.2 = (bf16[1024,2,1,64]{0,3,1,2:T(8,128)(2,1)}, bf16[1024,2,1,64]{0,3,1,2:T(8,128)(2,1)S(1)}, u32[]{:S(2)}) copy-start(bf16[1024,2,1,64]{0,3,1,2:T(8,128)(2,1)S(1)} %copy.98) | copy-start | bytes 786436 | tf_op jit(solution)/shard_map/while
  183.8 5.7 %copy-start.8 = (s32[6]{0:T(128)S(1)}, s32[6]{0:T(128)}, u32[]{:S(2)}) copy-start(s32[6]{0:T(128)} %get-tuple-element.259) | copy-start | bytes 76 | tf_op jit(solution)/shard_map/while
  183.8 7.6 %copy-start.6 = (bf16[1,128,512]{1,2,0:T(8,128)(2,1)S(1)}, bf16[1,128,512]{1,2,0:T(8,128)(2,1)}, u32[]{:S(2)}) copy-start(bf16[1,128,512]{1,2,0:T(8,128)(2,1)} %copy.96) | copy-start | bytes 393220 | tf_op jit(solution)/shard_map/while
  185.1 10.2 %copy-start.2 = (bf16[1024,2,1,64]{0,3,1,2:T(8,128)(2,1)}, bf16[1024,2,1,64]{0,3,1,2:T(8,128)(2,1)S(1)}, u32[]{:S(2)}) copy-start(bf16[1024,2,1,64]{0,3,1,2:T(8,128)(2,1)S(1)} %copy.98) | copy-start | bytes 786436 | tf_op jit(solution)/shard_map/while
  219.9 5.7 %copy-start.8 = (s32[6]{0:T(128)S(1)}, s32[6]{0:T(128)}, u32[]{:S(2)}) copy-start(s32[6]{0:T(128)} %get-tuple-element.259) | copy-start | bytes 76 | tf_op jit(solution)/shard_map/while
  219.9 7.6 %copy-start.6 = (bf16[1,128,512]{1,2,0:T(8,128)(2,1)S(1)}, bf16[1,128,512]{1,2,0:T(8,128)(2,1)}, u32[]{:S(2)}) copy-start(bf16[1,128,512]{1,2,0:T(8,128)(2,1)} %copy.96) | copy-start | bytes 393220 | tf_op jit(solution)/shard_map/while
  221.2 10.2 %copy-start.2 = (bf16[1024,2,1,64]{0,3,1,2:T(8,128)(2,1)}, bf16[1024,2,1,64]{0,3,1,2:T(8,128)(2,1)S(1)}, u32[]{:S(2)}) copy-start(bf16[1024,2,1,64]{0,3,1,2:T(8,128)(2,1)S(1)} %copy.98) | copy-start | bytes 786436 | tf_op jit(solution)/shard_map/while
  255.9 5.7 %copy-start.8 = (s32[6]{0:T(128)S(1)}, s32[6]{0:T(128)}, u32[]{:S(2)}) copy-start(s32[6]{0:T(128)} %get-tuple-element.259) | copy-start | bytes 76 | tf_op jit(solution)/shard_map/while
  255.9 7.6 %copy-start.6 = (bf16[1,128,512]{1,2,0:T(8,128)(2,1)S(1)}, bf16[1,128,512]{1,2,0:T(8,128)(2,1)}, u32[]{:S(2)}) copy-start(bf16[1,128,512]{1,2,0:T(8,128)(2,1)} %copy.96) | copy-start | bytes 393220 | tf_op jit(solution)/shard_map/while
  257.2 10.2 %copy-start.2 = (bf16[1024,2,1,64]{0,3,1,2:T(8,128)(2,1)}, bf16[1024,2,1,64]{0,3,1,2:T(8,128)(2,1)S(1)}, u32[]{:S(2)}) copy-start(bf16[1024,2,1,64]{0,3,1,2:T(8,128)(2,1)S(1)} %copy.98) | copy-start | bytes 786436 | tf_op jit(solution)/shard_map/while
  295.2 140.1 %all-to-all-start.2 = ((f32[8,6,64,256]{3,2,1,0:T(8,128)}), f32[8,6,64,256]{3,2,1,0:T(8,128)S(1)}, u32[]{:S(2)}, u32[]{:S(2)}) async-start(f32[8,6,64,256]{3,2,1,0:T(8,128)} %bitcast.38), calls=%async_computation.2 | async-start | bytes 6291456 | tf_op jit(solution)/shard_map/all_to_all | solution.py:102
  (18 other events, 40.6 us)
Sparse Core Ops, SparseCore 0:
  295.4 210.0 reduce-scatter.1
where the time goes:
time: 517 us; the launch traced here: 515 us
  waiting for transfers between devices  231 us (45%)
  local copies, waits for them, and re-layouts  113 us (22%)
  matrix products  95.9 us (19%)
  other arithmetic  33.7 us (7%)
  between operations  14.1 us (3%)
  blocking collectives  13.6 us (3%)
  starting transfers between devices  7.99 us (2%)
    all_to_all x1, waiting for transfers between devices, shards(): lax.all_to_all(grad_table.reshape(kv_count, capacity, BLK, row_width), 'k...  136 us
    reduce_scatter x1, waiting for transfers between devices, shards(): lax.psum_scatter(lax.dot_general(inputs, query_grad, (((0,), (0,)), ((),...  60.6 us
    all_to_all x1, waiting for transfers between devices, shards(): lax.all_to_all(fetched, 'kv', split_axis=0, concat_axis=0, tiled=True)  34.4 us
    reshape x12, local copies, waits for them, and re-layouts, one_block(): jnp.stack([key_part, value_part], axis=2).reshape(NSEL, BLK, row_width)  31.5 us
    dot_general x6, matrix products, one_block(): jnp.einsum('qhgn,qhgd->nhd', prob_round, grad_blk, preferred_element_type...  23.3 us
    dynamic_slice x30, local copies, waits for them, and re-layouts, shards(): grad_table, query_parts = lax.scan(one_block, start_table, packed)  22.8 us
    scatter-add x6, other arithmetic, one_block(): grad_table.at[slot_row].add(both_parts)  22.4 us
    dot_general x6, matrix products, one_block(): jnp.einsum('qhgd,nhd->qhgn', query_blk, key_blk, preferred_element_type=j...  22.1 us
  transfers between devices with their start and end apart: 3, of which 3 were waited for; matrix products, arithmetic and copies ran while one was open for 2% of the time, Pallas kernels for 0%

commit v1 on v0

v1 whole, which is shorter than its diff:
```python
import functools

import jax
import jax.numpy as jnp
from jax import lax
from jax.experimental import pallas as pl
from jax.experimental.pallas import tpu as pltpu
from jax.sharding import PartitionSpec as P


DH = 64
BLK = 64
QB = 128
NSEL = 16
ROW = 2 * DH


def attn_kernel(chosen_ref, slot_ref, first_ref, q_ref, o_ref, lse_ref, kv_ref, dq_ref, tab_ref,
                x, xt, kvg, p_s, d_s, ds_s, acc, *, nsel, group, at, cb, scale):
    i = pl.program_id(0)
    cols = group * QB
    keys = nsel * BLK

    @pl.when(i == 0)
    def _():
        acc[...] = jnp.zeros_like(acc)
        x[...] = jnp.zeros_like(x)
        xt[...] = jnp.zeros_like(xt)

    q = q_ref[...] * jnp.bfloat16(scale)
    o = o_ref[...]
    qt, ot = q.T, o.T
    for a in range(group):
        s = slice(a * DH, (a + 1) * DH)
        r = pl.ds(a * QB, QB)
        r2 = pl.ds(cols + a * QB, QB)
        x[r, pl.ds(0, DH)] = q[:, s]
        x[r2, pl.ds(DH, DH)] = o[:, s]
        xt[pl.ds(0, DH), r] = qt[s]
        xt[pl.ds(DH, DH), r2] = ot[s]
    lse_t = lse_ref[at * group:(at + 1) * group, :]
    start = (first_ref[0] + i) * QB
    slots, limits = [], []
    for j in range(nsel):
        c = chosen_ref[i * nsel + j]
        slots.append(jnp.where(c >= 0, slot_ref[jnp.maximum(c, 0)], 0))
        limits.append(jnp.where(c >= 0, start - c * BLK, -(1 << 28)))
    rows = lax.broadcasted_iota(jnp.int32, (BLK, QB), 0)
    lanes = lax.broadcasted_iota(jnp.int32, (BLK, QB), 1)
    gap = rows - lanes
    for j in range(nsel):
        s = slots[j]
        kvg[pl.ds(j * BLK, BLK), :] = kv_ref[pl.ds(pl.multiple_of(s * BLK, BLK), BLK), :]
    pair = 2 * QB
    crow = cb * BLK
    for h in range(cols // pair):
        dsum = jnp.zeros((8, pair), jnp.float32)
        lse = jnp.concatenate([lse_t[2 * h:2 * h + 1], lse_t[2 * h + 1:2 * h + 2]], axis=1)
        for c in range(keys // crow):
            kv_c = kvg[pl.ds(c * crow, crow), :]
            st = jnp.dot(kv_c, xt[:, pl.ds(h * pair, pair)], preferred_element_type=jnp.float32)
            dp = jnp.dot(kv_c, xt[:, pl.ds(cols + h * pair, pair)], preferred_element_type=jnp.float32)
            for b in range(cb):
                lim = limits[c * cb + b]
                seen = gap <= lim
                seen = jnp.concatenate([seen, seen], axis=1)
                sl = slice(b * BLK, (b + 1) * BLK)
                p = jnp.where(seen, jnp.exp(st[sl] - lse), 0.0)
                d = dp[sl]
                prod = p.astype(jnp.bfloat16).astype(jnp.float32) * d
                dsum = dsum + jnp.sum(prod.reshape(BLK // 8, 8, pair), axis=0)
                r = pl.ds(c * crow + b * BLK, BLK)
                p_s[r, pl.ds(h * pair, pair)] = p
                d_s[r, pl.ds(h * pair, pair)] = d
        delta = jnp.sum(dsum, axis=0, keepdims=True)
        for c in range(keys // crow):
            r = pl.ds(c * crow, crow)
            p = p_s[r, pl.ds(h * pair, pair)]
            d = d_s[r, pl.ds(h * pair, pair)]
            ds_s[r, pl.ds(h * pair, pair)] = (p * (d - delta)).astype(jnp.bfloat16)
            ds_s[r, pl.ds(cols + h * pair, pair)] = p.astype(jnp.bfloat16)
    for c in range(keys // crow):
        g = jnp.dot(ds_s[pl.ds(c * crow, crow), :], x[...], preferred_element_type=jnp.float32)
        for b in range(cb):
            s = slots[c * cb + b]
            r = pl.ds(pl.multiple_of(s * BLK, BLK), BLK)
            acc[r, :] += g[b * BLK:(b + 1) * BLK]
    kt = kvg[...].T[:DH]
    dqt = jnp.dot(kt, ds_s[:, pl.ds(0, cols)], preferred_element_type=jnp.float32)
    stack = jnp.concatenate([dqt[:, a * QB:(a + 1) * QB] for a in range(group)], axis=0)
    dq_ref[...] = (scale * stack.T).astype(dq_ref.dtype)

    @pl.when(i == pl.num_programs(0) - 1)
    def _():
        tab_ref[...] = acc[...].astype(tab_ref.dtype)


def attn(chosen, slots, first, queries, out_grad, log_sums, kv, *, nsel, group, at, cb=4):
    nq = queries.shape[0] // QB
    cols = group * QB
    wide = pl.BlockSpec((QB, group * DH), lambda i, *_: (i, at))
    return pl.pallas_call(
        functools.partial(
            attn_kernel, nsel=nsel, group=group, at=at, cb=cb, scale=DH ** (-0.5)
        ),
        grid_spec=pltpu.PrefetchScalarGridSpec(
            num_scalar_prefetch=3,
            grid=(nq,),
            in_specs=[
                wide,
                wide,
                pl.BlockSpec((log_sums.shape[0], QB), lambda i, *_: (0, i)),
                pl.BlockSpec(kv.shape, lambda i, *_: (0, 0)),
            ],
            out_specs=[
                pl.BlockSpec((QB, group * DH), lambda i, *_: (i, 0)),
                pl.BlockSpec(kv.shape, lambda i, *_: (0, 0)),
            ],
            scratch_shapes=[
                pltpu.VMEM((2 * cols, ROW), jnp.bfloat16),
                pltpu.VMEM((ROW, 2 * cols), jnp.bfloat16),
                pltpu.VMEM((nsel * BLK, ROW), jnp.bfloat16),
                pltpu.VMEM((nsel * BLK, cols), jnp.float32),
                pltpu.VMEM((nsel * BLK, cols), jnp.float32),
                pltpu.VMEM((nsel * BLK, 2 * cols), jnp.bfloat16),
                pltpu.VMEM(kv.shape, jnp.float32),
            ],
        ),
        out_shape=[
            jax.ShapeDtypeStruct((nq * QB, group * DH), jnp.bfloat16),
            jax.ShapeDtypeStruct(kv.shape, jnp.bfloat16),
        ],
        compiler_params=pltpu.CompilerParams(dimension_semantics=("arbitrary",)),
        cost_estimate=pl.CostEstimate(
            flops=nq * nsel * BLK * ROW * cols * 10,
            bytes_accessed=4 * kv.size + 8 * nq * QB * group * DH,
            transcendentals=nq * nsel * BLK * cols,
        ),
        name="attn_bwd",
    )(chosen, slots, first, queries, out_grad, log_sums, kv)


def sum_kernel(ask_ref, *refs):
    out_ref = refs[-1]
    out_ref[...] = jnp.zeros_like(out_ref)
    entries = refs[0].shape[0] // BLK
    for g, ref in enumerate(refs[:-1]):
        for j in range(entries):
            a = ask_ref[j]

            @pl.when(a >= 0)
            def _(g=g, ref=ref, j=j, a=a):
                r = pl.ds(pl.multiple_of(a * BLK, BLK), BLK)
                add = ref[pl.ds(j * BLK, BLK), :].astype(jnp.float32)
                out_ref[r, pl.ds(g * ROW, ROW)] += add


def sum_blocks(asked, parts, tok_count):
    vmem = pl.BlockSpec(memory_space=pltpu.VMEM)
    return pl.pallas_call(
        sum_kernel,
        in_specs=[pl.BlockSpec(memory_space=pltpu.SMEM)] + [vmem] * len(parts),
        out_specs=vmem,
        out_shape=jax.ShapeDtypeStruct((tok_count, ROW * len(parts)), jnp.float32),
        name="sum_blocks",
    )(asked, *parts)


def pack_kernel(*refs):
    out_ref = refs[-1]
    n = refs[0].shape[0]
    for k, ref in enumerate(refs[:-1]):
        out_ref[pl.ds(k * n, n), :] = ref[...]


def pack(parts):
    vmem = pl.BlockSpec(memory_space=pltpu.VMEM)
    shape = (parts[0].shape[0] * len(parts), parts[0].shape[1])
    return pl.pallas_call(
        pack_kernel,
        in_specs=[vmem] * len(parts),
        out_specs=vmem,
        out_shape=jax.ShapeDtypeStruct(shape, parts[0].dtype),
        name="pack",
    )(*parts)


def weight_kernel(place_ref, *refs, near):
    quarters, parts = refs[:4], refs[4:4 + near]
    own_ref, other_ref, rows_t = refs[4 + near:]
    tok = parts[0].shape[0]
    for k in range(near):
        rows_t[:, pl.ds(k * tok, tok)] = parts[k][...].T
    core, chip = place_ref[0], place_ref[1]
    size = quarters[0].shape[1]
    for k in range(4):
        t = jnp.dot(rows_t[...], quarters[k][...], preferred_element_type=jnp.float32).T
        away = core if k < 2 else 1 - core
        sub = chip if k % 2 == 0 else 1 - chip
        at = pl.ds(pl.multiple_of(sub * size, size), size)

        @pl.when(away == 0)
        def _():
            own_ref[at, :] = t

        @pl.when(away == 1)
        def _():
            other_ref[at, :] = t.astype(other_ref.dtype)


def weight_parts(place, quarters, parts):
    vmem = pl.BlockSpec(memory_space=pltpu.VMEM)
    near = len(parts)
    tok, cols = parts[0].shape
    shape = (2 * quarters[0].shape[1], cols)
    flops = 2 * near * tok * cols * 2 * shape[0]
    return pl.pallas_call(
        functools.partial(weight_kernel, near=near),
        in_specs=[pl.BlockSpec(memory_space=pltpu.SMEM)] + [vmem] * (4 + near),
        out_specs=[vmem, vmem],
        out_shape=[
            jax.ShapeDtypeStruct(shape, jnp.float32),
            jax.ShapeDtypeStruct(shape, jnp.bfloat16),
        ],
        scratch_shapes=[pltpu.VMEM((cols, near * tok), jnp.bfloat16)],
        cost_estimate=pl.CostEstimate(
            flops=flops, bytes_accessed=2 * 5 * quarters[0].size, transcendentals=0
        ),
        name="weight_parts",
    )(place, *quarters, *parts)


def exchange(x):
    return lax.all_to_all(x, "kv", split_axis=0, concat_axis=0, tiled=True)


def hop(x, step, axis="kv"):
    n = lax.axis_size(axis)
    return lax.ppermute(x, axis, [(j, j ^ step) for j in range(n)])


def input_slices(inputs, near, far):
    tok = inputs.shape[0]
    width = inputs.shape[1] // (near * far)
    me, at = lax.axis_index("kv"), lax.axis_index("tp")
    here, core, chip = me % near, at % 2, (at // 2) % 2
    half = far // 2
    side = ((me // near) % 2) ^ core
    slices = []
    for step in range(near):
        parts = []
        for f in range(max(half // 2, 1)):
            owner = side * half + chip * (half // 2) + f
            col = (owner * near + (here ^ step)) * width
            if half == 1:
                parts.append(lax.dynamic_slice(inputs, (0, col + chip * (width // 2)), (tok, width // 2)))
            else:
                parts.append(lax.dynamic_slice(inputs, (0, col), (tok, width)))
        slices.append(parts[0] if len(parts) == 1 else jnp.concatenate(parts, axis=1))
    return slices


def shards(queries, keys_values, log_sums, out_grad, inputs, chosen):
    tok_count = queries.shape[0]
    heads_here = queries.shape[1] // DH
    kv_heads = keys_values.shape[1] // ROW
    group = heads_here // kv_heads
    blocks_here = tok_count // BLK
    query_blocks = tok_count // QB
    kv_count = lax.axis_size("kv")
    near = 4
    far = kv_count // near
    me = lax.axis_index("kv")
    first_block = me * query_blocks
    capacity = blocks_here // 2
    total_blocks = kv_count * blocks_here

    flat_ids = chosen.reshape(-1)
    needed = jnp.any(
        flat_ids[:, None] == jnp.arange(total_blocks, dtype=jnp.int32)[None, :], axis=0
    )
    needed = needed.reshape(kv_count, blocks_here).astype(jnp.int32)
    rank_in = jnp.cumsum(needed, axis=1) - 1
    matches = (needed[:, :, None] == 1) & (
        rank_in[:, :, None] == jnp.arange(capacity, dtype=jnp.int32)[None, None, :]
    )
    request = jnp.sum(
        matches.astype(jnp.int32) * jnp.arange(blocks_here, dtype=jnp.int32)[None, :, None], axis=1
    )
    request = jnp.where(jnp.any(matches, axis=1), request, -1)
    slices = input_slices(inputs, near, far)
    asked = exchange(request)
    asked, slices = lax.optimization_barrier((asked, slices))
    asked = asked.reshape(-1)
    slots = jnp.arange(kv_count, dtype=jnp.int32)[:, None] * capacity + rank_in
    slots = jnp.clip(slots, 0, kv_count * capacity - 1).reshape(-1)
    first = first_block.astype(jnp.int32).reshape(1)
    flat_chosen = chosen.reshape(-1)
    lse = log_sums.T

    sends = []
    local_blocks = keys_values.reshape(blocks_here, BLK, kv_heads * ROW)
    picked = local_blocks[jnp.maximum(asked, 0)]
    for g in range(kv_heads):
        sends.append(picked[:, :, g * ROW : (g + 1) * ROW].reshape(kv_count, capacity * BLK, ROW))

    got = [slices[0]]
    for step in range(1, near):
        got.append(hop(slices[step], step))
    tables = []
    for g in range(kv_heads):
        tables.append(exchange(sends[g]).reshape(kv_count * capacity * BLK, ROW))

    dqs, returned, sums = [], [], []
    nears = []
    for g in range(kv_heads):
        dq, tab = attn(
            flat_chosen, slots, first, queries, out_grad, lse, tables[g],
            nsel=NSEL, group=group, at=g,
        )
        dqs.append(dq)
        nears.append([dq])
        for step in range(1, near):
            nears[g].append(hop(dq, step))
        back = exchange(tab.reshape(kv_count, capacity * BLK, ROW))
        returned.append(back.reshape(kv_count * capacity * BLK, ROW))
    seen = pack(got)
    beside = hop(seen, 2, "tp")
    twin = hop(seen, 1, "tp")
    beside_twin = hop(beside, 1, "tp")
    quarters = (seen, beside, twin, beside_twin)
    at = lax.axis_index("tp").astype(jnp.int32)
    place = jnp.stack([at % 2, (at // 2) % 2])
    width = inputs.shape[1] // kv_count
    for g in range(kv_heads):
        own, other = weight_parts(place, quarters, nears[g])
        cols = own.shape[1]
        if far == 2:
            other = hop(other, near)
            sums.append(own + other.astype(jnp.float32))
        else:
            even = (me // near) % 2 == 0
            own = own.astype(jnp.bfloat16)
            parts = jnp.concatenate([jnp.where(even, own, other), jnp.where(even, other, own)], axis=0)
            parts = parts.reshape(far, width, cols)
            groups = [[d + f * near for f in range(far)] for d in range(near)]
            parts = lax.all_to_all(
                parts, "kv", split_axis=0, concat_axis=0, tiled=True, axis_index_groups=groups
            )
            sums.append(jnp.sum(parts.astype(jnp.float32), axis=0))
    query_grad = jnp.concatenate(dqs, axis=1)
    kv_grad = sum_blocks(asked, returned, tok_count)
    weight_grad = jnp.concatenate(sums, axis=1)
    return (query_grad, kv_grad, weight_grad)


def solution(mesh):
    in_specs = (
        P("kv", "tp"),
        P("kv", "tp"),
        P("kv", "tp"),
        P("kv", "tp"),
        P("kv", None),
        P("kv", None),
    )
    out_specs = (P("kv", "tp"), P("kv", "tp"), P("kv", "tp"))
    return jax.shard_map(shards, mesh=mesh, in_specs=in_specs, out_specs=out_specs, check_vma=False)
```

time: 517 us -> 212 us (0.41)
  waiting for transfers between devices: 231 us -> 91.2 us
  local copies, waits for them, and re-layouts: 113 us -> 7.72 us
  matrix products: 95.9 us -> 0 us
  Pallas kernels: 0 us -> 53.8 us
  other arithmetic: 33.7 us -> 3.49 us
  starting transfers between devices: 7.99 us -> 32.3 us
  between operations: 14.1 us -> 0.78 us
  blocking collectives: 13.6 us -> 22.1 us
    all_to_all x2 -> x4, waiting for transfers between devices: 171 us -> 4.21 us  [exchange(): return lax.all_to_all(x, 'kv', split_axis=0, concat_axis=0, tiled=True)]
    dot_general x37 -> x0, matrix products: 95.9 us -> none  [the longest x6 23.3 us: one_block(): jnp.einsum('qhgn,qhgd->nhd', prob_round, grad_blk, preferred_element_type...]
    ppermute x0 -> x14, waiting for transfers between devices: none -> 87 us  [hop(): return lax.ppermute(x, axis, [(j, j ^ step) for j in range(n)])]
    reduce_scatter x1 -> x0, waiting for transfers between devices: 60.6 us -> none  [shards(): lax.psum_scatter(lax.dot_general(inputs, query_grad, (((0,), (0,)), ((),...]
    pallas_call x0 -> x6, Pallas kernels: none -> 53.8 us  [the longest x2 31.4 us: attn(): pl.pallas_call(functools.partial(attn_kernel, nsel=nsel, group=group, at=...]
    reshape x18 -> x2, local copies, waits for them, and re-layouts: 33.9 us -> 1.47 us  [the longest x1 0.81 us: shards(): flat_chosen = chosen.reshape(-1)]
    scatter-add x7 -> x0, other arithmetic: 29.1 us -> none  [the longest x6 22.4 us: one_block(): grad_table.at[slot_row].add(both_parts)]
    dynamic_slice x30 -> x1, local copies, waits for them, and re-layouts: 22.8 us -> 2.22 us  [input_slices(): lax.dynamic_slice(inputs, (0, col + chip * (width // 2)), (tok, width // 2))]
  transfers between devices with their start and end apart: 3 -> 18, of which waited for: 3 -> 10; matrix products, arithmetic and copies ran while one was open for 2% -> 2% of each run, Pallas kernels for 0% -> 25%
where the time goes in v1:
time: 212 us; the launch traced here: 211 us
  waiting for transfers between devices  91.2 us (43%)
  Pallas kernels  53.8 us (25%)
  starting transfers between devices  32.3 us (15%)
  blocking collectives  22.1 us (10%)
  local copies, waits for them, and re-layouts  7.72 us (4%)
  other arithmetic  3.49 us (2%)
    ppermute x14, waiting for transfers between devices, hop(): return lax.ppermute(x, axis, [(j, j ^ step) for j in range(n)])  87 us
    pallas_call x2, Pallas kernels, attn(): pl.pallas_call(functools.partial(attn_kernel, nsel=nsel, group=group, at=...  31.4 us
    all_to_all x1, blocking collectives, exchange(): return lax.all_to_all(x, 'kv', split_axis=0, concat_axis=0, tiled=True)  22.1 us
    all_to_all x4, starting transfers between devices, exchange(): return lax.all_to_all(x, 'kv', split_axis=0, concat_axis=0, tiled=True)  20.1 us
    pallas_call x2, Pallas kernels, weight_parts(): pl.pallas_call(functools.partial(weight_kernel, near=near), in_specs=[pl....  16.5 us
    ppermute x14, starting transfers between devices, hop(): return lax.ppermute(x, axis, [(j, j ^ step) for j in range(n)])  12.2 us
  transfers between devices with their start and end apart: 18, of which 10 were waited for; matrix products, arithmetic and copies ran while one was open for 2% of the time, Pallas kernels for 25%

profile of v1, /device:TPU:0, one launch (start us, length us, event | category | flops | bytes accessed | tf_op | source)
XLA Modules:
  0.0 211.5 jit_solution(15771931111914968116)
XLA Ops:
  3.0 7.3 %all-to-all-start = ((s32[8,1,6]{2,1,0:T(1,128)}), s32[8,1,6]{2,1,0:T(1,128)S(1)}, u32[]{:S(2)}, u32[]{:S(2)}) async-start(s32[8,1,6]{2,1,0:T(1,128)} %copy.11), calls=%async_computation | async-start | bytes 8192 | tf_op jit(solution)/shard_map/all_to_all | solution.py:234
  10.3 2.2 %constant_dynamic-slice_fusion = (bf16[768,256]{1,0:T(8,128)(2,1)S(1)}, bf16[768,256]{1,0:T(8,128)(2,1)S(1)}, bf16[768,256]{1,0:T(8,128)(2,1)}, bf16[768,256]{1,0:T(8,128)(2,1)S(1)}) fusion(bf16[768,4096]{1,0:T(8,128)(2,1)} %param.10, s32[]{:T(128)S(6)} %select_n.69, s32[]{:T(128)S(6)} %select_n.67, s32[]{:T(128)S(6)} %select_n.66, s32[]{:T(128)S(6)} %select_n.68), kind=kLoop, calls=%fused_computation.17 | loop fusion | bytes 3145744 | tf_op jit(solution)/shard_map/dynamic_slice | solution.py:256
  12.5 4.2 %all-to-all-done = s32[8,1,6]{2,1,0:T(1,128)S(1)} async-done(((s32[8,1,6]{2,1,0:T(1,128)}), s32[8,1,6]{2,1,0:T(1,128)S(1)}, u32[]{:S(2)}, u32[]{:S(2)}) %all-to-all-start) | async-done | bytes 224 | tf_op jit(solution)/shard_map/all_to_all | solution.py:234
  18.6 22.1 %all_to_all.29 = bf16[8,384,128]{2,1,0:T(8,128)(2,1)} all-to-all(bf16[8,384,128]{2,1,0:T(8,128)(2,1)S(1)} %bitcast.17), channel_id=1, replica_groups=mesh['kv'=8,'tp'=4] {'kv'}, dimensions={0} | all-to-all | bytes 1572864 | tf_op jit(solution)/shard_map/all_to_all | solution.py:234
  40.7 4.2 %all-to-all-start.2 = ((bf16[8,384,128]{2,1,0:T(8,128)(2,1)}), bf16[8,384,128]{2,1,0:T(8,128)(2,1)}, u32[]{:S(2)}, u32[]{:S(2)}) async-start(bf16[8,384,128]{2,1,0:T(8,128)(2,1)} %bitcast.7), calls=%async_computation.2 | async-start | bytes 1572864 | tf_op jit(solution)/shard_map/all_to_all | solution.py:234
  45.0 1.9 collective-permute-start
  48.5 14.6 %collective-permute-done.refs_1_ = bf16[768,256]{1,0:T(8,128)(2,1)S(1)} collective-permute-done((bf16[768,256]{1,0:T(8,128)(2,1)S(1)}, bf16[768,256]{1,0:T(8,128)(2,1)S(1)}, u32[]{:S(2)}, u32[]{:S(2)}) %collective-permute-start) | collective-permute-done | bytes 393248 | tf_op jit(solution)/shard_map/ppermute | solution.py:239
  63.1 6.6 %collective-permute-done.1.refs_2_ = bf16[768,256]{1,0:T(8,128)(2,1)S(1)} collective-permute-done((bf16[768,256]{1,0:T(8,128)(2,1)S(1)}, bf16[768,256]{1,0:T(8,128)(2,1)S(1)}, u32[]{:S(2)}, u32[]{:S(2)}) %collective-permute-start.1) | collective-permute-done | bytes 393248 | tf_op jit(solution)/shard_map/ppermute | solution.py:239
  69.7 7.0 %collective-permute-done.2.refs_3_ = bf16[768,256]{1,0:T(8,128)(2,1)S(1)} collective-permute-done((bf16[768,256]{1,0:T(8,128)(2,1)S(1)}, bf16[768,256]{1,0:T(8,128)(2,1)S(1)}, u32[]{:S(2)}, u32[]{:S(2)}) %collective-permute-start.2) | collective-permute-done | bytes 393248 | tf_op jit(solution)/shard_map/ppermute | solution.py:239
  77.4 2.6 %pack.1.refs_0_ = bf16[3072,256]{1,0:T(8,128)(2,1)} custom-call(bf16[768,256]{1,0:T(8,128)(2,1)} %get-tuple-element.21.refs_0_, bf16[768,256]{1,0:T(8,128)(2,1)} %copy-done.7, bf16[768,256]{1,0:T(8,128)(2,1)} %copy-done.8, bf16[768,256]{1,0:T(8,128)(2,1)} %copy-done.9), custom_call_target="tpu_custom_call" | custom-call | tf_op jit(solution)/shard_map/pack/pallas_call | solution.py:179
  82.1 15.7 %attn_bwd.2 = (bf16[768,256]{1,0:T(8,128)(2,1)}, bf16[3072,128]{1,0:T(8,128)(2,1)}) custom-call(s32[96]{0:T(128)} %copy-done.10, s32[96]{0:T(128)} %min.12.slot_ref, s32[1]{0:T(128)} %bitcast.first_ref, bf16[768,512]{1,0:T(8,128)(2,1)} %q_ref.3, bf16[768,512]{1,0:T(8,128)(2,1)} %o_ref.3, f32[8,768]{1,0:T(8,128)} %bitcast.23, bf16[3072,128]{1,0:T(8,128)(2,1)} %bitcast.19), custom_call_target="tpu_custom_call" | custom-call | flops 4026531840 | bytes 3145728 | tf_op jit(solution)/shard_map/attn_bwd/pallas_call | solution.py:102
  97.8 4.4 %all-to-all-start.3 = ((bf16[8,384,128]{2,1,0:T(8,128)(2,1)}), bf16[8,384,128]{2,1,0:T(8,128)(2,1)}, u32[]{:S(2)}, u32[]{:S(2)}) async-start(bf16[8,384,128]{2,1,0:T(8,128)(2,1)} %bitcast.20), calls=%async_computation.3 | async-start | bytes 1572864 | tf_op jit(solution)/shard_map/all_to_all | solution.py:234
  102.2 13.0 %collective-permute-done.3.refs_1_ = bf16[3072,256]{1,0:T(8,128)(2,1)S(1)} collective-permute-done((bf16[3072,256]{1,0:T(8,128)(2,1)}, bf16[3072,256]{1,0:T(8,128)(2,1)S(1)}, u32[]{:S(2)}, u32[]{:S(2)}) %collective-permute-start.3) | collective-permute-done | bytes 1572896 | tf_op jit(solution)/shard_map/ppermute | solution.py:239
  115.2 15.7 %attn_bwd.3 = (bf16[768,256]{1,0:T(8,128)(2,1)}, bf16[3072,128]{1,0:T(8,128)(2,1)}) custom-call(s32[96]{0:T(128)} %copy-done.10, s32[96]{0:T(128)} %min.12.slot_ref, s32[1]{0:T(128)} %bitcast.first_ref, bf16[768,512]{1,0:T(8,128)(2,1)} %q_ref.3, bf16[768,512]{1,0:T(8,128)(2,1)} %o_ref.3, f32[8,768]{1,0:T(8,128)} %bitcast.24, bf16[3072,128]{1,0:T(8,128)(2,1)} %bitcast.8.kv_ref), custom_call_target="tpu_custom_call" | custom-call | flops 4026531840 | bytes 3145728 | tf_op jit(solution)/shard_map/attn_bwd/pallas_call | solution.py:102
  130.9 4.2 %all-to-all-start.4 = ((bf16[8,384,128]{2,1,0:T(8,128)(2,1)}), bf16[8,384,128]{2,1,0:T(8,128)(2,1)}, u32[]{:S(2)}, u32[]{:S(2)}) async-start(bf16[8,384,128]{2,1,0:T(8,128)(2,1)} %bitcast.18), calls=%async_computation.4 | async-start | bytes 1572864 | tf_op jit(solution)/shard_map/all_to_all | solution.py:234
  135.2 1.9 collective-permute-start.10
  138.7 16.6 %collective-permute-done.10.refs_5_ = bf16[768,256]{1,0:T(8,128)(2,1)} collective-permute-done((bf16[768,256]{1,0:T(8,128)(2,1)}, bf16[768,256]{1,0:T(8,128)(2,1)}, u32[]{:S(2)}, u32[]{:S(2)}) %collective-permute-start.10) | collective-permute-done | bytes 393248 | tf_op jit(solution)/shard_map/ppermute | solution.py:239
  155.3 4.7 %collective-permute-done.11.refs_6_ = bf16[768,256]{1,0:T(8,128)(2,1)} collective-permute-done((bf16[768,256]{1,0:T(8,128)(2,1)}, bf16[768,256]{1,0:T(8,128)(2,1)}, u32[]{:S(2)}, u32[]{:S(2)}) %collective-permute-start.11) | collective-permute-done | bytes 393248 | tf_op jit(solution)/shard_map/ppermute | solution.py:239
  161.0 8.4 %collective-permute-done.12.refs_7_ = bf16[768,256]{1,0:T(8,128)(2,1)} collective-permute-done((bf16[768,256]{1,0:T(8,128)(2,1)}, bf16[768,256]{1,0:T(8,128)(2,1)}, u32[]{:S(2)}, u32[]{:S(2)}) %collective-permute-start.12) | collective-permute-done | bytes 393248 | tf_op jit(solution)/shard_map/ppermute | solution.py:239
  171.6 8.3 %weight_parts.3 = (f32[512,256]{1,0:T(8,128)}, bf16[512,256]{1,0:T(8,128)(2,1)}) custom-call(s32[2]{0:T(128)} %pad_add_fusion.place_ref, bf16[3072,256]{1,0:T(8,128)(2,1)} %pack.1.refs_0_, bf16[3072,256]{1,0:T(8,128)(2,1)} %copy-done.2, bf16[3072,256]{1,0:T(8,128)(2,1)} %collective-permute-done.4.refs_2_, bf16[3072,256]{1,0:T(8,128)(2,1)} %collective-permute-done.5.refs_3_, ...), custom_call_target="tpu_custom_call" | custom-call | flops 1610612736 | bytes 7864320 | tf_op jit(solution)/shard_map/weight_parts/pallas_call | solution.py:217
  181.5 8.7 %collective-permute-done.8.refs_7_ = bf16[768,256]{1,0:T(8,128)(2,1)} collective-permute-done((bf16[768,256]{1,0:T(8,128)(2,1)}, bf16[768,256]{1,0:T(8,128)(2,1)}, u32[]{:S(2)}, u32[]{:S(2)}) %collective-permute-start.8) | collective-permute-done | bytes 393248 | tf_op jit(solution)/shard_map/ppermute | solution.py:239
  190.3 8.2 %weight_parts.2 = (f32[512,256]{1,0:T(8,128)}, bf16[512,256]{1,0:T(8,128)(2,1)}) custom-call(s32[2]{0:T(128)} %pad_add_fusion.place_ref, bf16[3072,256]{1,0:T(8,128)(2,1)} %pack.1.refs_0_, bf16[3072,256]{1,0:T(8,128)(2,1)} %copy-done.2, bf16[3072,256]{1,0:T(8,128)(2,1)} %collective-permute-done.4.refs_2_, bf16[3072,256]{1,0:T(8,128)(2,1)} %collective-permute-done.5.refs_3_, ...), custom_call_target="tpu_custom_call" | custom-call | flops 1610612736 | bytes 7864320 | tf_op jit(solution)/shard_map/weight_parts/pallas_call | solution.py:217
  199.5 3.4 %sum_blocks.1 = f32[768,256]{1,0:T(8,128)} custom-call(s32[48]{0:T(128)} %reshape.104.ask_ref, bf16[3072,128]{1,0:T(8,128)(2,1)} %bitcast.10.refs_0_, bf16[3072,128]{1,0:T(8,128)(2,1)} %bitcast.12.refs_1_), custom_call_target="tpu_custom_call" | custom-call | tf_op jit(solution)/shard_map/sum_blocks/pallas_call | solution.py:160
  202.9 7.4 %collective-permute-done.9 = bf16[512,256]{1,0:T(8,128)(2,1)S(1)} collective-permute-done((bf16[512,256]{1,0:T(8,128)(2,1)}, bf16[512,256]{1,0:T(8,128)(2,1)S(1)}, u32[]{:S(2)}, u32[]{:S(2)}) %collective-permute-start.9) | collective-permute-done | bytes 262176 | tf_op jit(solution)/shard_map/ppermute | solution.py:239
  (66 shorter events, 17.4 us)
Async XLA Ops:
  0.6 16.2 %copy-start = (bf16[768,256]{1,0:T(8,128)(2,1)S(1)}, bf16[768,256]{1,0:T(8,128)(2,1)}, u32[]{:S(2)}) copy-start(bf16[768,256]{1,0:T(8,128)(2,1)} %param.7) | copy-start | bytes 1179652
  1.5 11.0 %copy-start.10 = (s32[96]{0:T(128)}, s32[96]{0:T(128)S(1)}, u32[]{:S(2)}) copy-start(s32[96]{0:T(128)S(1)} %reshape.97.chosen_ref) | copy-start | bytes 1156
  3.0 13.7 %all-to-all-start = ((s32[8,1,6]{2,1,0:T(1,128)}), s32[8,1,6]{2,1,0:T(1,128)S(1)}, u32[]{:S(2)}, u32[]{:S(2)}) async-start(s32[8,1,6]{2,1,0:T(1,128)} %copy.11), calls=%async_computation | async-start | bytes 8192 | tf_op jit(solution)/shard_map/all_to_all | solution.py:234
  40.7 57.0 %all-to-all-start.2 = ((bf16[8,384,128]{2,1,0:T(8,128)(2,1)}), bf16[8,384,128]{2,1,0:T(8,128)(2,1)}, u32[]{:S(2)}, u32[]{:S(2)}) async-start(bf16[8,384,128]{2,1,0:T(8,128)(2,1)} %bitcast.7), calls=%async_computation.2 | async-start | bytes 1572864 | tf_op jit(solution)/shard_map/all_to_all | solution.py:234
  45.0 18.1 %collective-permute-start = (bf16[768,256]{1,0:T(8,128)(2,1)S(1)}, bf16[768,256]{1,0:T(8,128)(2,1)S(1)}, u32[]{:S(2)}, u32[]{:S(2)}) collective-permute-start(bf16[768,256]{1,0:T(8,128)(2,1)S(1)} %get-tuple-element.22), channel_id=1, source_target_pairs={{0,4},{4,0},{8,12},{12,8},{16,20},{20,16},{24,28},{28,24},{1,5},{5... | collective-permute-start | bytes 1179656 | tf_op jit(solution)/shard_map/ppermute | solution.py:239
  46.9 22.8 %collective-permute-start.1 = (bf16[768,256]{1,0:T(8,128)(2,1)S(1)}, bf16[768,256]{1,0:T(8,128)(2,1)S(1)}, u32[]{:S(2)}, u32[]{:S(2)}) collective-permute-start(bf16[768,256]{1,0:T(8,128)(2,1)S(1)} %get-tuple-element.23), channel_id=1, source_target_pairs={{0,8},{4,12},{8,0},{12,4},{16,24},{20,28},{24,16},{28,20},{1,9},{5... | collective-permute-start | bytes 1179656 | tf_op jit(solution)/shard_map/ppermute | solution.py:239
  48.3 28.3 %collective-permute-start.2 = (bf16[768,256]{1,0:T(8,128)(2,1)S(1)}, bf16[768,256]{1,0:T(8,128)(2,1)S(1)}, u32[]{:S(2)}, u32[]{:S(2)}) collective-permute-start(bf16[768,256]{1,0:T(8,128)(2,1)S(1)} %get-tuple-element.24), channel_id=1, source_target_pairs={{0,12},{4,8},{8,4},{12,0},{16,28},{20,24},{24,20},{28,16},{1,13},{... | collective-permute-start | bytes 1179656 | tf_op jit(solution)/shard_map/ppermute | solution.py:239
  63.1 13.5 %copy-start.7 = (bf16[768,256]{1,0:T(8,128)(2,1)}, bf16[768,256]{1,0:T(8,128)(2,1)S(1)}, u32[]{:S(2)}) copy-start(bf16[768,256]{1,0:T(8,128)(2,1)S(1)} %collective-permute-done.refs_1_) | copy-start | bytes 1179652
  80.0 35.3 %collective-permute-start.3 = (bf16[3072,256]{1,0:T(8,128)(2,1)}, bf16[3072,256]{1,0:T(8,128)(2,1)S(1)}, u32[]{:S(2)}, u32[]{:S(2)}) collective-permute-start(bf16[3072,256]{1,0:T(8,128)(2,1)} %pack.1.refs_0_), channel_id=1, source_target_pairs={{0,2},{1,3},{2,0},{3,1},{4,6},{5,7},{6,4},{7,5},{8,10},{9,11},{10,... | collective-permute-start | bytes 4718600 | tf_op jit(solution)/shard_map/ppermute | solution.py:239
  97.8 33.2 %all-to-all-start.3 = ((bf16[8,384,128]{2,1,0:T(8,128)(2,1)}), bf16[8,384,128]{2,1,0:T(8,128)(2,1)}, u32[]{:S(2)}, u32[]{:S(2)}) async-start(bf16[8,384,128]{2,1,0:T(8,128)(2,1)} %bitcast.20), calls=%async_computation.3 | async-start | bytes 1572864 | tf_op jit(solution)/shard_map/all_to_all | solution.py:234
  102.1 69.5 %collective-permute-start.4 = (bf16[3072,256]{1,0:T(8,128)(2,1)S(1)}, bf16[3072,256]{1,0:T(8,128)(2,1)}, u32[]{:S(2)}, u32[]{:S(2)}) collective-permute-start(bf16[3072,256]{1,0:T(8,128)(2,1)S(1)} %copy-done.1), channel_id=1, source_target_pairs={{0,1},{1,0},{2,3},{3,2},{4,5},{5,4},{6,7},{7,6},{8,9},{9,8},{10,11... | collective-permute-start | bytes 4718600 | tf_op jit(solution)/shard_map/ppermute | solution.py:239
  115.2 15.7 %copy-start.2 = (bf16[3072,256]{1,0:T(8,128)(2,1)}, bf16[3072,256]{1,0:T(8,128)(2,1)S(1)}, u32[]{:S(2)}) copy-start(bf16[3072,256]{1,0:T(8,128)(2,1)S(1)} %collective-permute-done.3.refs_1_) | copy-start | bytes 4718596
  115.2 56.4 %collective-permute-start.5 = (bf16[3072,256]{1,0:T(8,128)(2,1)S(1)}, bf16[3072,256]{1,0:T(8,128)(2,1)}, u32[]{:S(2)}, u32[]{:S(2)}) collective-permute-start(bf16[3072,256]{1,0:T(8,128)(2,1)S(1)} %collective-permute-done.3.refs_1_), channel_id=1, source_target_pairs={{0,1},{1,0},{2,3},{3,2},{4,5},{5,4},{6,7},{7,6},{8,9},{9,8},{10,11... | collective-permute-start | bytes 4718600 | tf_op jit(solution)/shard_map/ppermute | solution.py:239
  130.9 68.5 %all-to-all-start.4 = ((bf16[8,384,128]{2,1,0:T(8,128)(2,1)}), bf16[8,384,128]{2,1,0:T(8,128)(2,1)}, u32[]{:S(2)}, u32[]{:S(2)}) async-start(bf16[8,384,128]{2,1,0:T(8,128)(2,1)} %bitcast.18), calls=%async_computation.4 | async-start | bytes 1572864 | tf_op jit(solution)/shard_map/all_to_all | solution.py:234
  135.2 20.1 %collective-permute-start.10 = (bf16[768,256]{1,0:T(8,128)(2,1)}, bf16[768,256]{1,0:T(8,128)(2,1)}, u32[]{:S(2)}, u32[]{:S(2)}) collective-permute-start(bf16[768,256]{1,0:T(8,128)(2,1)} %get-tuple-element.18.refs_4_), channel_id=1, source_target_pairs={{0,4},{4,0},{8,12},{12,8},{16,20},{20,16},{24,28},{28,24},{1,5},{5... | collective-permute-start | bytes 1179656 | tf_op jit(solution)/shard_map/ppermute | solution.py:239
  137.1 23.0 %collective-permute-start.11 = (bf16[768,256]{1,0:T(8,128)(2,1)}, bf16[768,256]{1,0:T(8,128)(2,1)}, u32[]{:S(2)}, u32[]{:S(2)}) collective-permute-start(bf16[768,256]{1,0:T(8,128)(2,1)} %get-tuple-element.18.refs_4_), channel_id=1, source_target_pairs={{0,8},{4,12},{8,0},{12,4},{16,24},{20,28},{24,16},{28,20},{1,9},{5... | collective-permute-start | bytes 1179656 | tf_op jit(solution)/shard_map/ppermute | solution.py:239
  138.6 30.9 %collective-permute-start.12 = (bf16[768,256]{1,0:T(8,128)(2,1)}, bf16[768,256]{1,0:T(8,128)(2,1)}, u32[]{:S(2)}, u32[]{:S(2)}) collective-permute-start(bf16[768,256]{1,0:T(8,128)(2,1)} %get-tuple-element.18.refs_4_), channel_id=1, source_target_pairs={{0,12},{4,8},{8,4},{12,0},{16,28},{20,24},{24,20},{28,16},{1,13},{... | collective-permute-start | bytes 1179656 | tf_op jit(solution)/shard_map/ppermute | solution.py:239
  155.3 26.2 %collective-permute-start.6 = (bf16[768,256]{1,0:T(8,128)(2,1)}, bf16[768,256]{1,0:T(8,128)(2,1)}, u32[]{:S(2)}, u32[]{:S(2)}) collective-permute-start(bf16[768,256]{1,0:T(8,128)(2,1)} %get-tuple-element.17.refs_4_), channel_id=1, source_target_pairs={{0,4},{4,0},{8,12},{12,8},{16,20},{20,16},{24,28},{28,24},{1,5},{5... | collective-permute-start | bytes 1179656 | tf_op jit(solution)/shard_map/ppermute | solution.py:239
  160.0 21.5 %collective-permute-start.7 = (bf16[768,256]{1,0:T(8,128)(2,1)}, bf16[768,256]{1,0:T(8,128)(2,1)}, u32[]{:S(2)}, u32[]{:S(2)}) collective-permute-start(bf16[768,256]{1,0:T(8,128)(2,1)} %get-tuple-element.17.refs_4_), channel_id=1, source_target_pairs={{0,8},{4,12},{8,0},{12,4},{16,24},{20,28},{24,16},{28,20},{1,9},{5... | collective-permute-start | bytes 1179656 | tf_op jit(solution)/shard_map/ppermute | solution.py:239
  169.4 20.9 %collective-permute-start.8 = (bf16[768,256]{1,0:T(8,128)(2,1)}, bf16[768,256]{1,0:T(8,128)(2,1)}, u32[]{:S(2)}, u32[]{:S(2)}) collective-permute-start(bf16[768,256]{1,0:T(8,128)(2,1)} %get-tuple-element.17.refs_4_), channel_id=1, source_target_pairs={{0,12},{4,8},{8,4},{12,0},{16,28},{20,24},{24,20},{28,16},{1,13},{... | collective-permute-start | bytes 1179656 | tf_op jit(solution)/shard_map/ppermute | solution.py:239
  179.9 18.6 %copy-start.3 = (bf16[768,256]{1,0:T(8,128)(2,1)S(1)}, bf16[768,256]{1,0:T(8,128)(2,1)}, u32[]{:S(2)}) copy-start(bf16[768,256]{1,0:T(8,128)(2,1)} %get-tuple-element.17.refs_4_) | copy-start | bytes 1179652
  179.9 18.6 %copy-start.4 = (bf16[768,256]{1,0:T(8,128)(2,1)S(1)}, bf16[768,256]{1,0:T(8,128)(2,1)}, u32[]{:S(2)}) copy-start(bf16[768,256]{1,0:T(8,128)(2,1)} %get-tuple-element.18.refs_4_) | copy-start | bytes 1179652
  179.9 23.0 %collective-permute-start.13 = (bf16[512,256]{1,0:T(8,128)(2,1)}, bf16[512,256]{1,0:T(8,128)(2,1)S(1)}, u32[]{:S(2)}, u32[]{:S(2)}) collective-permute-start(bf16[512,256]{1,0:T(8,128)(2,1)} %get-tuple-element.28), channel_id=1, source_target_pairs={{0,16},{4,20},{8,24},{12,28},{16,0},{20,4},{24,8},{28,12},{1,17},{... | collective-permute-start | bytes 786440 | tf_op jit(solution)/shard_map/ppermute | solution.py:239
  198.5 11.8 %collective-permute-start.9 = (bf16[512,256]{1,0:T(8,128)(2,1)}, bf16[512,256]{1,0:T(8,128)(2,1)S(1)}, u32[]{:S(2)}, u32[]{:S(2)}) collective-permute-start(bf16[512,256]{1,0:T(8,128)(2,1)} %get-tuple-element.26), channel_id=1, source_target_pairs={{0,16},{4,20},{8,24},{12,28},{16,0},{20,4},{24,8},{28,12},{1,17},{... | collective-permute-start | bytes 786440 | tf_op jit(solution)/shard_map/ppermute | solution.py:239
  (5 other events, 26.3 us)

commit v2 on v1

v2 whole, which is shorter than its diff:
```python
import functools

import jax
import jax.numpy as jnp
from jax import lax
from jax.experimental import pallas as pl
from jax.experimental.pallas import tpu as pltpu
from jax.sharding import PartitionSpec as P


DH = 64
BLK = 64
QB = 128
NSEL = 16
ROW = 2 * DH


def attn_kernel(chosen_ref, slot_ref, first_ref, q_ref, o_ref, lse_ref, kv_ref, dq_ref, tab_ref,
                x, xt, kvg, p_s, d_s, ds_s, acc, *, nsel, group, at, unroll, scale):
    i = pl.program_id(0)
    cols = group * QB
    pair = 2 * QB

    @pl.when(i == 0)
    def _():
        acc[...] = jnp.zeros_like(acc)
        x[...] = jnp.zeros_like(x)
        xt[...] = jnp.zeros_like(xt)

    gap = lax.broadcasted_iota(jnp.int32, (BLK, QB), 0) - lax.broadcasted_iota(
        jnp.int32, (BLK, QB), 1
    )

    def prepare(u):
        q = q_ref[pl.ds(u * QB, QB), :] * jnp.bfloat16(scale)
        o = o_ref[pl.ds(u * QB, QB), :]
        qt, ot = q.T, o.T
        for a in range(group):
            s = slice(a * DH, (a + 1) * DH)
            r = pl.ds(a * QB, QB)
            r2 = pl.ds(cols + a * QB, QB)
            x[u, r, pl.ds(0, DH)] = q[:, s]
            x[u, r2, pl.ds(DH, DH)] = o[:, s]
            xt[u, pl.ds(0, DH), r] = qt[s]
            xt[u, pl.ds(DH, DH), r2] = ot[s]
        block = i * unroll + u
        start = (first_ref[0] + block) * QB
        slots, limits = [], []
        for j in range(nsel):
            c = chosen_ref[block * nsel + j]
            slots.append(jnp.where(c >= 0, slot_ref[jnp.maximum(c, 0)], 0))
            limits.append(jnp.where(c >= 0, start - c * BLK, -(1 << 28)))
        for j in range(nsel):
            r = pl.ds(pl.multiple_of(slots[j] * BLK, BLK), BLK)
            kvg[u, pl.ds(j * BLK, BLK), :] = kv_ref[r, :]
        return slots, limits

    def scores(u, h, limits):
        top = lse_ref[at * group + 2 * h:at * group + 2 * h + 1, pl.ds(u * QB, QB)]
        low_row = lse_ref[at * group + 2 * h + 1:at * group + 2 * h + 2, pl.ds(u * QB, QB)]
        lse = jnp.concatenate([top, low_row], axis=1)
        here = pl.ds(h * pair, pair)
        there = pl.ds(cols + h * pair, pair)
        st = jnp.dot(kvg[u], xt[u, :, here], preferred_element_type=jnp.float32)
        dp = jnp.dot(kvg[u], xt[u, :, there], preferred_element_type=jnp.float32)
        part = jnp.zeros((8, pair), jnp.float32)
        for j in range(nsel):
            seen = gap <= limits[j]
            seen = jnp.concatenate([seen, seen], axis=1)
            sl = slice(j * BLK, (j + 1) * BLK)
            p = jnp.where(seen, jnp.exp(st[sl] - lse), 0.0)
            d = dp[sl]
            low = p.astype(jnp.bfloat16)
            prod = low.astype(jnp.float32) * d
            part = part + jnp.sum(prod.reshape(BLK // 8, 8, pair), axis=0)
            r = pl.ds(j * BLK, BLK)
            p_s[u, r, here] = p
            d_s[u, r, here] = d
            ds_s[u, r, there] = low
        return jnp.sum(part, axis=0, keepdims=True)

    def grads(u, slots, deltas):
        for h in range(cols // pair):
            here = pl.ds(h * pair, pair)
            ds_s[u, :, here] = (p_s[u, :, here] * (d_s[u, :, here] - deltas[h])).astype(jnp.bfloat16)
        kt = kvg[u].T[:DH]
        dqt = jnp.dot(kt, ds_s[u, :, pl.ds(0, cols)], preferred_element_type=jnp.float32)
        g = jnp.dot(ds_s[u], x[u], preferred_element_type=jnp.float32)
        for j in range(nsel):
            r = pl.ds(pl.multiple_of(slots[j] * BLK, BLK), BLK)
            acc[r, :] += g[j * BLK:(j + 1) * BLK]
        stack = jnp.concatenate([dqt[:, a * QB:(a + 1) * QB] for a in range(group)], axis=0)
        dq_ref[pl.ds(u * QB, QB), :] = (scale * stack.T).astype(dq_ref.dtype)

    blocks = [prepare(u) for u in range(unroll)]
    deltas = [[scores(u, h, blocks[u][1]) for h in range(cols // pair)] for u in range(unroll)]
    for u in range(unroll):
        grads(u, blocks[u][0], deltas[u])

    @pl.when(i == pl.num_programs(0) - 1)
    def _():
        tab_ref[...] = acc[...].astype(tab_ref.dtype)


def attn(chosen, slots, first, queries, out_grad, log_sums, kv, *, nsel, group, at):
    nq = queries.shape[0] // QB
    unroll = next(u for u in (3, 2, 1) if nq % u == 0)
    cols = group * QB
    rows = unroll * QB
    wide = pl.BlockSpec((rows, group * DH), lambda i, *_: (i, at))
    return pl.pallas_call(
        functools.partial(
            attn_kernel, nsel=nsel, group=group, at=at, unroll=unroll, scale=DH ** (-0.5)
        ),
        grid_spec=pltpu.PrefetchScalarGridSpec(
            num_scalar_prefetch=3,
            grid=(nq // unroll,),
            in_specs=[
                wide,
                wide,
                pl.BlockSpec((log_sums.shape[0], rows), lambda i, *_: (0, i)),
                pl.BlockSpec(kv.shape, lambda i, *_: (0, 0)),
            ],
            out_specs=[
                pl.BlockSpec((rows, group * DH), lambda i, *_: (i, 0)),
                pl.BlockSpec(kv.shape, lambda i, *_: (0, 0)),
            ],
            scratch_shapes=[
                pltpu.VMEM((unroll, 2 * cols, ROW), jnp.bfloat16),
                pltpu.VMEM((unroll, ROW, 2 * cols), jnp.bfloat16),
                pltpu.VMEM((unroll, nsel * BLK, ROW), jnp.bfloat16),
                pltpu.VMEM((unroll, nsel * BLK, cols), jnp.float32),
                pltpu.VMEM((unroll, nsel * BLK, cols), jnp.float32),
                pltpu.VMEM((unroll, nsel * BLK, 2 * cols), jnp.bfloat16),
                pltpu.VMEM(kv.shape, jnp.float32),
            ],
        ),
        out_shape=[
            jax.ShapeDtypeStruct((nq * QB, group * DH), jnp.bfloat16),
            jax.ShapeDtypeStruct(kv.shape, jnp.bfloat16),
        ],
        compiler_params=pltpu.CompilerParams(dimension_semantics=("arbitrary",)),
        cost_estimate=pl.CostEstimate(
            flops=nq * nsel * BLK * ROW * cols * 10,
            bytes_accessed=4 * kv.size + 8 * nq * QB * group * DH,
            transcendentals=nq * nsel * BLK * cols,
        ),
        name="attn_bwd",
    )(chosen, slots, first, queries, out_grad, log_sums, kv)


def pick_kernel(ids_ref, own_ref, away_ref, out_ref):
    edge = own_ref.shape[0] // BLK
    for j in range(out_ref.shape[0] // BLK):
        at = jnp.maximum(ids_ref[j], 0)

        @pl.when(at < edge)
        def _(j=j, at=at):
            r = pl.ds(pl.multiple_of(at * BLK, BLK), BLK)
            out_ref[pl.ds(j * BLK, BLK), :] = own_ref[r, :]

        @pl.when(at >= edge)
        def _(j=j, at=at):
            r = pl.ds(pl.multiple_of((at - edge) * BLK, BLK), BLK)
            out_ref[pl.ds(j * BLK, BLK), :] = away_ref[r, :]


def pick_blocks(ids, own, away):
    vmem = pl.BlockSpec(memory_space=pltpu.VMEM)
    return pl.pallas_call(
        pick_kernel,
        in_specs=[pl.BlockSpec(memory_space=pltpu.SMEM), vmem, vmem],
        out_specs=vmem,
        out_shape=jax.ShapeDtypeStruct((ids.shape[0] * BLK, own.shape[1]), own.dtype),
        name="pick_blocks",
    )(ids, own, away)


def sum_kernel(ids_ref, in_ref, own_ref, away_ref, acc):
    edge = own_ref.shape[0]
    acc[...] = jnp.zeros_like(acc)
    for j in range(in_ref.shape[0] // BLK):
        at = ids_ref[j]

        @pl.when(at >= 0)
        def _(j=j, at=at):
            r = pl.ds(pl.multiple_of(at * BLK, BLK), BLK)
            acc[r, :] += in_ref[pl.ds(j * BLK, BLK), :].astype(jnp.float32)

    own_ref[...] = acc[pl.ds(0, edge), :]
    away_ref[...] = acc[pl.ds(edge, away_ref.shape[0]), :].astype(away_ref.dtype)


def sum_blocks(ids, back, own_rows, away_rows):
    vmem = pl.BlockSpec(memory_space=pltpu.VMEM)
    width = back.shape[1]
    return pl.pallas_call(
        sum_kernel,
        in_specs=[pl.BlockSpec(memory_space=pltpu.SMEM), vmem],
        out_specs=[vmem, vmem],
        out_shape=[
            jax.ShapeDtypeStruct((own_rows, width), jnp.float32),
            jax.ShapeDtypeStruct((away_rows, width), jnp.bfloat16),
        ],
        scratch_shapes=[pltpu.VMEM((own_rows + away_rows, width), jnp.float32)],
        name="sum_blocks",
    )(ids, back)


def pack_kernel(*refs):
    n = (len(refs) - 3)
    sources, out_ref = refs[:n], refs[n]
    buf, sems = refs[n + 1:]
    tok = buf.shape[1]
    ins = [pltpu.make_async_copy(sources[k], buf.at[k], sems.at[k]) for k in range(n)]
    outs = [
        pltpu.make_async_copy(buf.at[k], out_ref.at[pl.ds(k * tok, tok), :], sems.at[n + k])
        for k in range(n)
    ]
    for copy in ins:
        copy.start()
    for k in range(n):
        ins[k].wait()
        outs[k].start()
    for copy in outs:
        copy.wait()


def pack(parts):
    hbm = pl.BlockSpec(memory_space=pl.ANY)
    n = len(parts)
    shape = (parts[0].shape[0] * n, parts[0].shape[1])
    return pl.pallas_call(
        pack_kernel,
        in_specs=[hbm] * n,
        out_specs=hbm,
        out_shape=jax.ShapeDtypeStruct(shape, parts[0].dtype),
        scratch_shapes=[
            pltpu.VMEM((n,) + parts[0].shape, parts[0].dtype),
            pltpu.SemaphoreType.DMA((2 * n,)),
        ],
        name="pack",
    )(*parts)


def weight_kernel(place_ref, inputs_ref, *refs, near, pieces):
    sources = refs[:4 + near]
    own_ref, other_ref, rows_t, parts, quarters, sems = refs[4 + near:]
    tok = parts.shape[1]
    size = sources[0].shape[1]
    copies = [
        pltpu.make_async_copy(sources[4 + k], parts.at[k], sems.at[k]) for k in range(near)
    ]
    local, rest = [], []
    for k in range(4):
        for f in range(pieces):
            col = pl.ds(pl.multiple_of(place_ref[2 + k * pieces + f], 128), size // pieces)
            to = quarters.at[pl.ds(0, tok), pl.ds(k * size + f * (size // pieces), size // pieces)]
            at = near + 4 + k * pieces + f
            local.append(pltpu.make_async_copy(inputs_ref.at[:, col], to, sems.at[at]))
        to = quarters.at[pl.ds(tok, (near - 1) * tok), pl.ds(k * size, size)]
        rest.append(pltpu.make_async_copy(sources[k], to, sems.at[near + k]))
    for copy in copies:
        copy.start()
    for k in range(4):
        for copy in local[k * pieces:(k + 1) * pieces]:
            copy.start()
        rest[k].start()
    for k in range(near):
        copies[k].wait()
        rows_t[:, pl.ds(k * tok, tok)] = parts[k].T
    core, chip = place_ref[0], place_ref[1]
    for pair in range(2):
        for k in (2 * pair, 2 * pair + 1):
            rest[k].wait()
            for copy in local[k * pieces:(k + 1) * pieces]:
                copy.wait()
        both = jnp.dot(
            rows_t[...],
            quarters[:, pl.ds(pair * 2 * size, 2 * size)],
            preferred_element_type=jnp.float32,
        )
        away = core if pair == 0 else 1 - core
        for k in range(2):
            t = both[:, k * size:(k + 1) * size].T
            sub = chip if k == 0 else 1 - chip
            at = pl.ds(pl.multiple_of(sub * size, size), size)

            @pl.when(away == 0)
            def _(t=t, at=at):
                own_ref[at, :] = t

            @pl.when(away == 1)
            def _(t=t, at=at):
                other_ref[at, :] = t.astype(other_ref.dtype)


def weight_parts(place, inputs, quarters, parts):
    vmem = pl.BlockSpec(memory_space=pltpu.VMEM)
    near = len(parts)
    tok, cols = parts[0].shape
    size = quarters[0].shape[1]
    pieces = (place.shape[0] - 2) // 4
    flops = 2 * near * tok * cols * 4 * size
    return pl.pallas_call(
        functools.partial(weight_kernel, near=near, pieces=pieces),
        in_specs=[pl.BlockSpec(memory_space=pltpu.SMEM)]
        + [pl.BlockSpec(memory_space=pl.ANY)] * (5 + near),
        out_specs=[vmem, vmem],
        out_shape=[
            jax.ShapeDtypeStruct((2 * size, cols), jnp.float32),
            jax.ShapeDtypeStruct((2 * size, cols), jnp.bfloat16),
        ],
        scratch_shapes=[
            pltpu.VMEM((cols, near * tok), jnp.bfloat16),
            pltpu.VMEM((near, tok, cols), jnp.bfloat16),
            pltpu.VMEM((near * tok, 4 * size), jnp.bfloat16),
            pltpu.SemaphoreType.DMA((near + 4 + 4 * pieces,)),
        ],
        cost_estimate=pl.CostEstimate(
            flops=flops, bytes_accessed=2 * 6 * quarters[0].size, transcendentals=0
        ),
        name="weight_parts",
    )(place, inputs, *quarters, *parts)


def exchange(x, groups):
    return lax.all_to_all(
        x, "kv", split_axis=0, concat_axis=0, tiled=True, axis_index_groups=groups
    )


def hop(x, step, axis="kv"):
    n = lax.axis_size(axis)
    return lax.ppermute(x, axis, [(j, j ^ step) for j in range(n)])


def column_starts(width, near, far, here, core, chip):
    half = far // 2
    side = ((lax.axis_index("kv") // near) % 2) ^ core
    if half == 1:
        return [(side * near + here) * width + chip * (width // 2)], width // 2
    owners = [side * half + chip * (half // 2) + f for f in range(half // 2)]
    return [(owner * near + here) * width for owner in owners], width


def input_slices(inputs, near, far):
    tok = inputs.shape[0]
    width = inputs.shape[1] // (near * far)
    here, at = lax.axis_index("kv") % near, lax.axis_index("tp")
    slices = []
    for step in range(1, near):
        cols, size = column_starts(width, near, far, here ^ step, at % 2, (at // 2) % 2)
        parts = [lax.dynamic_slice(inputs, (0, col), (tok, size)) for col in cols]
        slices.append(parts[0] if len(parts) == 1 else jnp.concatenate(parts, axis=1))
    return slices


def shards(queries, keys_values, log_sums, out_grad, inputs, chosen):
    tok_count = queries.shape[0]
    heads_here = queries.shape[1] // DH
    kv_heads = keys_values.shape[1] // ROW
    group = heads_here // kv_heads
    blocks_here = tok_count // BLK
    query_blocks = tok_count // QB
    kv_count = lax.axis_size("kv")
    near = 4
    far = kv_count // near
    me = lax.axis_index("kv")
    first_block = me * query_blocks
    capacity = blocks_here // 2
    total_blocks = kv_count * blocks_here

    flat_ids = chosen.reshape(-1)
    needed = jnp.any(
        flat_ids[:, None] == jnp.arange(total_blocks, dtype=jnp.int32)[None, :], axis=0
    )
    needed = needed.reshape(kv_count, blocks_here).astype(jnp.int32)
    rank_in = jnp.cumsum(needed, axis=1) - 1
    matches = (needed[:, :, None] == 1) & (
        rank_in[:, :, None] == jnp.arange(capacity, dtype=jnp.int32)[None, None, :]
    )
    request = jnp.sum(
        matches.astype(jnp.int32) * jnp.arange(blocks_here, dtype=jnp.int32)[None, :, None], axis=1
    )
    request = jnp.where(jnp.any(matches, axis=1), request, -1)
    request = jnp.swapaxes(request.reshape(far, near, capacity), 0, 1)
    near_groups = [[f * near + d for d in range(near)] for f in range(far)]
    far_groups = [[f * near + d for f in range(far)] for d in range(near)]
    far_at = me // near

    slices = input_slices(inputs, near, far)
    heads_kv = [keys_values[:, g * ROW : (g + 1) * ROW] for g in range(kv_heads)]
    away_kv = []
    for g in range(kv_heads):
        if far == 2:
            away_kv.append(lax.ppermute(heads_kv[g], "kv", [(j, j + near) for j in range(near)]))
        else:
            away_kv.append(
                lax.all_gather(heads_kv[g], "kv", tiled=True, axis_index_groups=far_groups)
            )
    asked = exchange(request, near_groups)
    owner = jnp.arange(far, dtype=jnp.int32)
    offset = ((owner != far_at) if far == 2 else owner + 1).astype(jnp.int32) * blocks_here
    ids = jnp.where(asked >= 0, asked + offset[None, :, None], -1).reshape(-1)
    of_block = jnp.arange(total_blocks, dtype=jnp.int32) // blocks_here
    slots = ((of_block % near) * far + of_block // near) * capacity + rank_in.reshape(-1)
    slots = jnp.clip(slots, 0, kv_count * capacity - 1)
    first = first_block.astype(jnp.int32).reshape(1)
    flat_chosen = chosen.reshape(-1)
    lse = log_sums.T

    tables = []
    for g in range(kv_heads):
        send = pick_blocks(ids, heads_kv[g], away_kv[g])
        table = exchange(send.reshape(near, -1, ROW), near_groups)
        tables.append(table.reshape(kv_count * capacity * BLK, ROW))
    got = []
    for step in range(1, near):
        got.append(hop(slices[step - 1], step))

    dqs, returned, sums = [], [], []
    nears = []
    for g in range(kv_heads):
        dq, tab = attn(
            flat_chosen, slots, first, queries, out_grad, lse, tables[g],
            nsel=NSEL, group=group, at=g,
        )
        dqs.append(dq)
        nears.append([dq])
        for step in range(1, near):
            relay = g == kv_heads - 1 and step == 3
            nears[g].append(hop(nears[g][2], 1) if relay else hop(dq, step))
        back = exchange(tab.reshape(near, -1, ROW), near_groups)
        returned.append(back.reshape(kv_count * capacity * BLK, ROW))
    seen = pack(got)
    beside = hop(seen, 2, "tp")
    twin = hop(seen, 1, "tp")
    beside_twin = hop(beside, 1, "tp")
    quarters = (seen, beside, twin, beside_twin)
    at = lax.axis_index("tp").astype(jnp.int32)
    core, chip = at % 2, (at // 2) % 2
    width = inputs.shape[1] // kv_count
    entries = [core, chip]
    for k in range(4):
        cols, _ = column_starts(width, near, far, me % near, core ^ (k // 2), chip ^ (k % 2))
        entries += cols
    place = jnp.stack([jnp.asarray(e, jnp.int32) for e in entries])
    for g in range(kv_heads):
        own, other = weight_parts(place, inputs, quarters, nears[g])
        cols = own.shape[1]
        if far == 2:
            other = hop(other, near)
            sums.append(own + other.astype(jnp.float32))
        else:
            even = (me // near) % 2 == 0
            own = own.astype(jnp.bfloat16)
            parts = jnp.concatenate([jnp.where(even, own, other), jnp.where(even, other, own)], axis=0)
            parts = parts.reshape(far, width, cols)
            parts = exchange(parts, far_groups)
            sums.append(jnp.sum(parts.astype(jnp.float32), axis=0))
    query_grad = jnp.concatenate(dqs, axis=1)
    kv_parts = []
    for g in range(kv_heads):
        own, away = sum_blocks(ids, returned[g], tok_count, tok_count * (1 if far == 2 else far))
        if far == 2:
            away = lax.ppermute(away, "kv", [(j + near, j) for j in range(near)])
            kv_parts.append(own + away.astype(jnp.float32))
        else:
            away = exchange(away.reshape(far, tok_count, ROW), far_groups)
            kv_parts.append(own + jnp.sum(away.astype(jnp.float32), axis=0))
    kv_grad = jnp.concatenate(kv_parts, axis=1)
    weight_grad = jnp.concatenate(sums, axis=1)
    return (query_grad, kv_grad, weight_grad)


def solution(mesh):
    in_specs = (
        P("kv", "tp"),
        P("kv", "tp"),
        P("kv", "tp"),
        P("kv", "tp"),
        P("kv", None),
        P("kv", None),
    )
    out_specs = (P("kv", "tp"), P("kv", "tp"), P("kv", "tp"))
    return jax.shard_map(shards, mesh=mesh, in_specs=in_specs, out_specs=out_specs, check_vma=False)
```

time: 212 us -> 180 us (0.85)
  waiting for transfers between devices: 91.2 us -> 56.8 us
  starting transfers between devices: 32.3 us -> 56.5 us
  blocking collectives: 22.1 us -> 0 us
  Pallas kernels: 53.8 us -> 51.5 us
    ppermute x14, waiting for transfers between devices: 87 us -> 37.3 us  [hop(): return lax.ppermute(x, axis, [(j, j ^ step) for j in range(n)])]
    all_to_all x1 -> x0, blocking collectives: 22.1 us -> none  [exchange(): return lax.all_to_all(x, 'kv', split_axis=0, concat_axis=0, tiled=True)]
    ppermute x0 -> x4, waiting for transfers between devices: none -> 19.5 us  [the longest x2 11 us: shards(): lax.ppermute(heads_kv[g], 'kv', [(j, j + near) for j in range(near)])]
    ppermute x0 -> x4, starting transfers between devices: none -> 12.4 us  [the longest x2 9.79 us: shards(): lax.ppermute(heads_kv[g], 'kv', [(j, j + near) for j in range(near)])]
    all_to_all x4 -> x5, starting transfers between devices: 20.1 us -> 26.2 us  [exchange(): lax.all_to_all(x, 'kv', split_axis=0, concat_axis=0, tiled=True, axis_ind...]
    ppermute x14, starting transfers between devices: 12.2 us -> 17.9 us  [hop(): return lax.ppermute(x, axis, [(j, j ^ step) for j in range(n)])]
    pallas_call x2, Pallas kernels: 31.4 us -> 26.4 us  [attn(): pl.pallas_call(functools.partial(attn_kernel, nsel=nsel, group=group, at=...]
    all_to_all x4 -> x5, waiting for transfers between devices: 4.21 us -> 0.01 us  [exchange(): lax.all_to_all(x, 'kv', split_axis=0, concat_axis=0, tiled=True, axis_ind...]
  transfers between devices with their start and end apart: 18 -> 23, of which waited for: 10 -> 10; matrix products, arithmetic and copies ran while one was open for 2% -> 5% of each run, Pallas kernels for 25% -> 27%
where the time goes in v2:
time: 180 us; the launch traced here: 179 us
  waiting for transfers between devices  56.8 us (32%)
  starting transfers between devices  56.5 us (31%)
  Pallas kernels  51.5 us (29%)
  local copies, waits for them, and re-layouts  8.08 us (4%)
  other arithmetic  5.56 us (3%)
    ppermute x14, waiting for transfers between devices, hop(): return lax.ppermute(x, axis, [(j, j ^ step) for j in range(n)])  37.3 us
    pallas_call x2, Pallas kernels, attn(): pl.pallas_call(functools.partial(attn_kernel, nsel=nsel, group=group, at=...  26.4 us
    all_to_all x5, starting transfers between devices, exchange(): lax.all_to_all(x, 'kv', split_axis=0, concat_axis=0, tiled=True, axis_ind...  26.2 us
    ppermute x14, starting transfers between devices, hop(): return lax.ppermute(x, axis, [(j, j ^ step) for j in range(n)])  17.9 us
    pallas_call x2, Pallas kernels, weight_parts(): pl.pallas_call(functools.partial(weight_kernel, near=near, pieces=pieces)...  12.9 us
    ppermute x2, waiting for transfers between devices, shards(): lax.ppermute(heads_kv[g], 'kv', [(j, j + near) for j in range(near)])  11 us
    ppermute x2, starting transfers between devices, shards(): lax.ppermute(heads_kv[g], 'kv', [(j, j + near) for j in range(near)])  9.79 us
    ppermute x2, waiting for transfers between devices, shards(): away = lax.ppermute(away, 'kv', [(j + near, j) for j in range(near)])  8.54 us
  transfers between devices with their start and end apart: 23, of which 10 were waited for; matrix products, arithmetic and copies ran while one was open for 5% of the time, Pallas kernels for 27%

profile of v2, /device:TPU:0, one launch (start us, length us, event | category | flops | bytes accessed | tf_op | source)
XLA Modules:
  0.0 179.3 jit_solution(12604215878829703103)
XLA Ops:
  2.8 5.3 %all-to-all-start = ((s32[4,2,6]{2,1,0:T(2,128)}), s32[4,2,6]{2,1,0:T(2,128)S(1)}, u32[]{:S(2)}, u32[]{:S(2)}) async-start(s32[4,2,6]{2,1,0:T(2,128)} %copy.12), calls=%async_computation | async-start | bytes 8192 | tf_op jit(solution)/shard_map/all_to_all | solution.py:328
  9.2 4.5 %collective-permute-start.1 = (bf16[768,128]{1,0:T(8,128)(2,1)S(1)}, bf16[768,128]{1,0:T(8,128)(2,1)S(1)}, u32[]{:S(2)}, u32[]{:S(2)}) collective-permute-start(bf16[768,128]{1,0:T(8,128)(2,1)S(1)} %get-tuple-element.31.own_ref), channel_id=1, source_target_pairs={{0,16},{4,20},{8,24},{12,28},{1,17},{5,21},{9,25},{13,29},{2,18},{... | collective-permute-start | bytes 589832 | tf_op jit(solution)/shard_map/ppermute | solution.py:397
  14.4 3.2 %collective-permute-done.1.away_ref = bf16[768,128]{1,0:T(8,128)(2,1)S(1)} collective-permute-done((bf16[768,128]{1,0:T(8,128)(2,1)S(1)}, bf16[768,128]{1,0:T(8,128)(2,1)S(1)}, u32[]{:S(2)}, u32[]{:S(2)}) %collective-permute-start.1) | collective-permute-done | bytes 196640 | tf_op jit(solution)/shard_map/ppermute | solution.py:397
  18.3 2.6 %pick_blocks.3 = bf16[3072,128]{1,0:T(8,128)(2,1)} custom-call(s32[48]{0:T(128)} %reshape.69.ids_ref, bf16[768,128]{1,0:T(8,128)(2,1)} %copy-done.7, bf16[768,128]{1,0:T(8,128)(2,1)} %copy-done.15), custom_call_target="tpu_custom_call" | custom-call | tf_op jit(solution)/shard_map/pick_blocks/pallas_call | solution.py:170
  20.9 8.1 %all-to-all-start.2 = ((bf16[4,768,128]{2,1,0:T(8,128)(2,1)}), bf16[4,768,128]{2,1,0:T(8,128)(2,1)S(1)}, u32[]{:S(2)}, u32[]{:S(2)}) async-start(bf16[4,768,128]{2,1,0:T(8,128)(2,1)} %bitcast.21), calls=%async_computation.2 | async-start | bytes 1572864 | tf_op jit(solution)/shard_map/all_to_all | solution.py:328
  28.9 5.3 %collective-permute-start = (bf16[768,128]{1,0:T(8,128)(2,1)S(1)}, bf16[768,128]{1,0:T(8,128)(2,1)S(1)}, u32[]{:S(2)}, u32[]{:S(2)}) collective-permute-start(bf16[768,128]{1,0:T(8,128)(2,1)S(1)} %get-tuple-element.30.own_ref), channel_id=1, source_target_pairs={{0,16},{4,20},{8,24},{12,28},{1,17},{5,21},{9,25},{13,29},{2,18},{... | collective-permute-start | bytes 589832 | tf_op jit(solution)/shard_map/ppermute | solution.py:397
  34.2 7.8 %collective-permute-done.away_ref = bf16[768,128]{1,0:T(8,128)(2,1)S(1)} collective-permute-done((bf16[768,128]{1,0:T(8,128)(2,1)S(1)}, bf16[768,128]{1,0:T(8,128)(2,1)S(1)}, u32[]{:S(2)}, u32[]{:S(2)}) %collective-permute-start) | collective-permute-done | bytes 196640 | tf_op jit(solution)/shard_map/ppermute | solution.py:397
  42.7 2.6 %pick_blocks.2 = bf16[3072,128]{1,0:T(8,128)(2,1)} custom-call(s32[48]{0:T(128)} %reshape.69.ids_ref, bf16[768,128]{1,0:T(8,128)(2,1)} %copy-done.6, bf16[768,128]{1,0:T(8,128)(2,1)} %copy-done.16), custom_call_target="tpu_custom_call" | custom-call | tf_op jit(solution)/shard_map/pick_blocks/pallas_call | solution.py:170
  45.3 4.5 %all-to-all-start.1 = ((bf16[4,768,128]{2,1,0:T(8,128)(2,1)}), bf16[4,768,128]{2,1,0:T(8,128)(2,1)S(1)}, u32[]{:S(2)}, u32[]{:S(2)}) async-start(bf16[4,768,128]{2,1,0:T(8,128)(2,1)} %bitcast.19), calls=%async_computation.1 | async-start | bytes 1572864 | tf_op jit(solution)/shard_map/all_to_all | solution.py:328
  55.9 13.2 %attn_bwd.3 = (bf16[768,256]{1,0:T(8,128)(2,1)}, bf16[3072,128]{1,0:T(8,128)(2,1)}) custom-call(s32[96]{0:T(128)} %copy-done.17, s32[96]{0:T(128)} %add_clamp_fusion.slot_ref, s32[1]{0:T(128)} %bitcast.first_ref, bf16[768,512]{1,0:T(8,128)(2,1)} %q_ref.3, bf16[768,512]{1,0:T(8,128)(2,1)} %o_ref.3, f32[8,768]{1,0:T(8,128)} %bitcast.27, bf16[3072,128]{1,0:T(8,128)(2,1)} %bitcast.23), custom_call_target="tpu_custom_call" | custom-call | flops 4026531840 | bytes 3145728 | tf_op jit(solution)/shard_map/attn_bwd/pallas_call | solution.py:111
  69.2 4.2 %all-to-all-start.4 = ((bf16[4,768,128]{2,1,0:T(8,128)(2,1)}), bf16[4,768,128]{2,1,0:T(8,128)(2,1)S(1)}, u32[]{:S(2)}, u32[]{:S(2)}) async-start(bf16[4,768,128]{2,1,0:T(8,128)(2,1)} %bitcast.25), calls=%async_computation.4 | async-start | bytes 1572864 | tf_op jit(solution)/shard_map/all_to_all | solution.py:328
  73.4 6.4 %collective-permute-done.6.refs_2_ = bf16[768,256]{1,0:T(8,128)(2,1)S(1)} collective-permute-done((bf16[768,256]{1,0:T(8,128)(2,1)S(1)}, bf16[768,256]{1,0:T(8,128)(2,1)S(1)}, u32[]{:S(2)}, u32[]{:S(2)}) %collective-permute-start.6) | collective-permute-done | bytes 393248 | tf_op jit(solution)/shard_map/ppermute | solution.py:335
  84.2 13.2 %attn_bwd.2 = (bf16[768,256]{1,0:T(8,128)(2,1)}, bf16[3072,128]{1,0:T(8,128)(2,1)}) custom-call(s32[96]{0:T(128)} %copy-done.17, s32[96]{0:T(128)} %add_clamp_fusion.slot_ref, s32[1]{0:T(128)} %bitcast.first_ref, bf16[768,512]{1,0:T(8,128)(2,1)} %q_ref.3, bf16[768,512]{1,0:T(8,128)(2,1)} %o_ref.3, f32[8,768]{1,0:T(8,128)} %bitcast.28, bf16[3072,128]{1,0:T(8,128)(2,1)} %bitcast.22), custom_call_target="tpu_custom_call" | custom-call | flops 4026531840 | bytes 3145728 | tf_op jit(solution)/shard_map/attn_bwd/pallas_call | solution.py:111
  97.4 4.2 %all-to-all-start.3 = ((bf16[4,768,128]{2,1,0:T(8,128)(2,1)}), bf16[4,768,128]{2,1,0:T(8,128)(2,1)}, u32[]{:S(2)}, u32[]{:S(2)}) async-start(bf16[4,768,128]{2,1,0:T(8,128)(2,1)} %bitcast.24), calls=%async_computation.3 | async-start | bytes 1572864 | tf_op jit(solution)/shard_map/all_to_all | solution.py:328
  101.6 3.7 %collective-permute-done.7.refs_1_ = bf16[2304,256]{1,0:T(8,128)(2,1)S(1)} collective-permute-done((bf16[2304,256]{1,0:T(8,128)(2,1)}, bf16[2304,256]{1,0:T(8,128)(2,1)S(1)}, u32[]{:S(2)}, u32[]{:S(2)}) %collective-permute-start.7) | collective-permute-done | bytes 1179680 | tf_op jit(solution)/shard_map/ppermute | solution.py:335
  106.5 15.4 %collective-permute-done.15.refs_6_ = bf16[768,256]{1,0:T(8,128)(2,1)} collective-permute-done((bf16[768,256]{1,0:T(8,128)(2,1)}, bf16[768,256]{1,0:T(8,128)(2,1)}, u32[]{:S(2)}, u32[]{:S(2)}) %collective-permute-start.15) | collective-permute-done | bytes 393248 | tf_op jit(solution)/shard_map/ppermute | solution.py:335
  124.2 2.6 %collective-permute-start.12 = (bf16[768,256]{1,0:T(8,128)(2,1)}, bf16[768,256]{1,0:T(8,128)(2,1)}, u32[]{:S(2)}, u32[]{:S(2)}) collective-permute-start(bf16[768,256]{1,0:T(8,128)(2,1)} %get-tuple-element.15.refs_4_), channel_id=1, source_target_pairs={{0,12},{4,8},{8,4},{12,0},{16,28},{20,24},{24,20},{28,16},{1,13},{... | collective-permute-start | bytes 1179656 | tf_op jit(solution)/shard_map/ppermute | solution.py:335
  137.6 6.4 %weight_parts.3 = (f32[512,256]{1,0:T(8,128)}, bf16[512,256]{1,0:T(8,128)(2,1)}) custom-call(s32[6]{0:T(128)} %stack.27.place_ref, bf16[768,4096]{1,0:T(8,128)(2,1)} %inputs_ref.3, bf16[2304,256]{1,0:T(8,128)(2,1)} %pack.1.refs_0_, bf16[2304,256]{1,0:T(8,128)(2,1)} %copy-done, bf16[2304,256]{1,0:T(8,128)(2,1)} %copy-done.1, bf16[2304,256]{1,0:T(8,128)(2,1)} %copy-done.2, ...), custom_call_target="tpu_custom_call" | custom-call | flops 1610612736 | bytes 7077888 | tf_op jit(solution)/shard_map/weight_parts/pallas_call | solution.py:305
  144.0 2.6 %collective-permute-done.10.refs_5_ = bf16[768,256]{1,0:T(8,128)(2,1)} collective-permute-done((bf16[768,256]{1,0:T(8,128)(2,1)}, bf16[768,256]{1,0:T(8,128)(2,1)}, u32[]{:S(2)}, u32[]{:S(2)}) %collective-permute-start.10) | collective-permute-done | bytes 393248 | tf_op jit(solution)/shard_map/ppermute | solution.py:335
  146.6 6.5 %collective-permute-start.17 = (bf16[512,256]{1,0:T(8,128)(2,1)}, bf16[512,256]{1,0:T(8,128)(2,1)S(1)}, u32[]{:S(2)}, u32[]{:S(2)}) collective-permute-start(bf16[512,256]{1,0:T(8,128)(2,1)} %get-tuple-element.26), channel_id=1, source_target_pairs={{0,16},{4,20},{8,24},{12,28},{16,0},{20,4},{24,8},{28,12},{1,17},{... | collective-permute-start | bytes 786440 | tf_op jit(solution)/shard_map/ppermute | solution.py:335
  153.2 6.5 %weight_parts.2 = (f32[512,256]{1,0:T(8,128)}, bf16[512,256]{1,0:T(8,128)(2,1)}) custom-call(s32[6]{0:T(128)} %stack.27.place_ref, bf16[768,4096]{1,0:T(8,128)(2,1)} %inputs_ref.3, bf16[2304,256]{1,0:T(8,128)(2,1)} %pack.1.refs_0_, bf16[2304,256]{1,0:T(8,128)(2,1)} %copy-done, bf16[2304,256]{1,0:T(8,128)(2,1)} %copy-done.1, bf16[2304,256]{1,0:T(8,128)(2,1)} %copy-done.2, ...), custom_call_target="tpu_custom_call" | custom-call | flops 1610612736 | bytes 7077888 | tf_op jit(solution)/shard_map/weight_parts/pallas_call | solution.py:305
  159.9 8.5 %collective-permute-done.2 = bf16[768,128]{1,0:T(8,128)(2,1)S(1)} collective-permute-done((bf16[768,128]{1,0:T(8,128)(2,1)}, bf16[768,128]{1,0:T(8,128)(2,1)S(1)}, u32[]{:S(2)}, u32[]{:S(2)}) %collective-permute-start.2) | collective-permute-done | bytes 196640 | tf_op jit(solution)/shard_map/ppermute | solution.py:467
  169.4 4.6 %collective-permute-done.17 = bf16[512,256]{1,0:T(8,128)(2,1)S(1)} collective-permute-done((bf16[512,256]{1,0:T(8,128)(2,1)}, bf16[512,256]{1,0:T(8,128)(2,1)S(1)}, u32[]{:S(2)}, u32[]{:S(2)}) %collective-permute-start.17) | collective-permute-done | bytes 262176 | tf_op jit(solution)/shard_map/ppermute | solution.py:335
  174.1 4.0 %collective-permute-done.13 = bf16[512,256]{1,0:T(8,128)(2,1)S(1)} collective-permute-done((bf16[512,256]{1,0:T(8,128)(2,1)}, bf16[512,256]{1,0:T(8,128)(2,1)S(1)}, u32[]{:S(2)}, u32[]{:S(2)}) %collective-permute-start.13) | collective-permute-done | bytes 262176 | tf_op jit(solution)/shard_map/ppermute | solution.py:335
  (94 shorter events, 32.6 us)
Async XLA Ops:
  2.8 10.9 %all-to-all-start = ((s32[4,2,6]{2,1,0:T(2,128)}), s32[4,2,6]{2,1,0:T(2,128)S(1)}, u32[]{:S(2)}, u32[]{:S(2)}) async-start(s32[4,2,6]{2,1,0:T(2,128)} %copy.12), calls=%async_computation | async-start | bytes 8192 | tf_op jit(solution)/shard_map/all_to_all | solution.py:328
  9.2 32.8 %copy-start.6 = (bf16[768,128]{1,0:T(8,128)(2,1)}, bf16[768,128]{1,0:T(8,128)(2,1)S(1)}, u32[]{:S(2)}) copy-start(bf16[768,128]{1,0:T(8,128)(2,1)S(1)} %get-tuple-element.30.own_ref) | copy-start | bytes 589828
  9.2 8.4 %collective-permute-start.1 = (bf16[768,128]{1,0:T(8,128)(2,1)S(1)}, bf16[768,128]{1,0:T(8,128)(2,1)S(1)}, u32[]{:S(2)}, u32[]{:S(2)}) collective-permute-start(bf16[768,128]{1,0:T(8,128)(2,1)S(1)} %get-tuple-element.31.own_ref), channel_id=1, source_target_pairs={{0,16},{4,20},{8,24},{12,28},{1,17},{5,21},{9,25},{13,29},{2,18},{... | collective-permute-start | bytes 589832 | tf_op jit(solution)/shard_map/ppermute | solution.py:397
  20.9 24.4 %all-to-all-start.2 = ((bf16[4,768,128]{2,1,0:T(8,128)(2,1)}), bf16[4,768,128]{2,1,0:T(8,128)(2,1)S(1)}, u32[]{:S(2)}, u32[]{:S(2)}) async-start(bf16[4,768,128]{2,1,0:T(8,128)(2,1)} %bitcast.21), calls=%async_computation.2 | async-start | bytes 1572864 | tf_op jit(solution)/shard_map/all_to_all | solution.py:328
  28.9 13.1 %collective-permute-start = (bf16[768,128]{1,0:T(8,128)(2,1)S(1)}, bf16[768,128]{1,0:T(8,128)(2,1)S(1)}, u32[]{:S(2)}, u32[]{:S(2)}) collective-permute-start(bf16[768,128]{1,0:T(8,128)(2,1)S(1)} %get-tuple-element.30.own_ref), channel_id=1, source_target_pairs={{0,16},{4,20},{8,24},{12,28},{1,17},{5,21},{9,25},{13,29},{2,18},{... | collective-permute-start | bytes 589832 | tf_op jit(solution)/shard_map/ppermute | solution.py:397
  45.3 23.9 %all-to-all-start.1 = ((bf16[4,768,128]{2,1,0:T(8,128)(2,1)}), bf16[4,768,128]{2,1,0:T(8,128)(2,1)S(1)}, u32[]{:S(2)}, u32[]{:S(2)}) async-start(bf16[4,768,128]{2,1,0:T(8,128)(2,1)} %bitcast.19), calls=%async_computation.1 | async-start | bytes 1572864 | tf_op jit(solution)/shard_map/all_to_all | solution.py:328
  51.8 21.5 %collective-permute-start.4 = (bf16[768,256]{1,0:T(8,128)(2,1)}, bf16[768,256]{1,0:T(8,128)(2,1)S(1)}, u32[]{:S(2)}, u32[]{:S(2)}) collective-permute-start(bf16[768,256]{1,0:T(8,128)(2,1)} %get-tuple-element.29), channel_id=1, source_target_pairs={{0,4},{4,0},{8,12},{12,8},{16,20},{20,16},{24,28},{28,24},{1,5},{5... | collective-permute-start | bytes 1179656 | tf_op jit(solution)/shard_map/ppermute | solution.py:335
  53.8 19.5 %collective-permute-start.5 = (bf16[768,256]{1,0:T(8,128)(2,1)S(1)}, bf16[768,256]{1,0:T(8,128)(2,1)S(1)}, u32[]{:S(2)}, u32[]{:S(2)}) collective-permute-start(bf16[768,256]{1,0:T(8,128)(2,1)S(1)} %get-tuple-element.28), channel_id=1, source_target_pairs={{0,8},{4,12},{8,0},{12,4},{16,24},{20,28},{24,16},{28,20},{1,9},{5... | collective-permute-start | bytes 1179656 | tf_op jit(solution)/shard_map/ppermute | solution.py:335
  55.3 24.4 %collective-permute-start.6 = (bf16[768,256]{1,0:T(8,128)(2,1)S(1)}, bf16[768,256]{1,0:T(8,128)(2,1)S(1)}, u32[]{:S(2)}, u32[]{:S(2)}) collective-permute-start(bf16[768,256]{1,0:T(8,128)(2,1)S(1)} %get-tuple-element.27), channel_id=1, source_target_pairs={{0,12},{4,8},{8,4},{12,0},{16,28},{20,24},{24,20},{28,16},{1,13},{... | collective-permute-start | bytes 1179656 | tf_op jit(solution)/shard_map/ppermute | solution.py:335
  69.2 28.2 %all-to-all-start.4 = ((bf16[4,768,128]{2,1,0:T(8,128)(2,1)}), bf16[4,768,128]{2,1,0:T(8,128)(2,1)S(1)}, u32[]{:S(2)}, u32[]{:S(2)}) async-start(bf16[4,768,128]{2,1,0:T(8,128)(2,1)} %bitcast.25), calls=%async_computation.4 | async-start | bytes 1572864 | tf_op jit(solution)/shard_map/all_to_all | solution.py:328
  82.6 22.7 %collective-permute-start.7 = (bf16[2304,256]{1,0:T(8,128)(2,1)}, bf16[2304,256]{1,0:T(8,128)(2,1)S(1)}, u32[]{:S(2)}, u32[]{:S(2)}) collective-permute-start(bf16[2304,256]{1,0:T(8,128)(2,1)} %pack.1.refs_0_), channel_id=1, source_target_pairs={{0,2},{1,3},{2,0},{3,1},{4,6},{5,7},{6,4},{7,5},{8,10},{9,11},{10,... | collective-permute-start | bytes 3538952 | tf_op jit(solution)/shard_map/ppermute | solution.py:335
  84.2 39.7 %collective-permute-start.8 = (bf16[2304,256]{1,0:T(8,128)(2,1)}, bf16[2304,256]{1,0:T(8,128)(2,1)S(1)}, u32[]{:S(2)}, u32[]{:S(2)}) collective-permute-start(bf16[2304,256]{1,0:T(8,128)(2,1)} %pack.1.refs_0_), channel_id=1, source_target_pairs={{0,1},{1,0},{2,3},{3,2},{4,5},{5,4},{6,7},{7,6},{8,9},{9,8},{10,11... | collective-permute-start | bytes 3538952 | tf_op jit(solution)/shard_map/ppermute | solution.py:335
  97.4 34.6 %all-to-all-start.3 = ((bf16[4,768,128]{2,1,0:T(8,128)(2,1)}), bf16[4,768,128]{2,1,0:T(8,128)(2,1)}, u32[]{:S(2)}, u32[]{:S(2)}) async-start(bf16[4,768,128]{2,1,0:T(8,128)(2,1)} %bitcast.24), calls=%async_computation.3 | async-start | bytes 1572864 | tf_op jit(solution)/shard_map/all_to_all | solution.py:328
  105.3 30.9 %collective-permute-start.9 = (bf16[2304,256]{1,0:T(8,128)(2,1)S(1)}, bf16[2304,256]{1,0:T(8,128)(2,1)S(1)}, u32[]{:S(2)}, u32[]{:S(2)}) collective-permute-start(bf16[2304,256]{1,0:T(8,128)(2,1)S(1)} %collective-permute-done.7.refs_1_), channel_id=1, source_target_pairs={{0,1},{1,0},{2,3},{3,2},{4,5},{5,4},{6,7},{7,6},{8,9},{9,8},{10,11... | collective-permute-start | bytes 3538952 | tf_op jit(solution)/shard_map/ppermute | solution.py:335
  105.3 16.5 %collective-permute-start.15 = (bf16[768,256]{1,0:T(8,128)(2,1)}, bf16[768,256]{1,0:T(8,128)(2,1)}, u32[]{:S(2)}, u32[]{:S(2)}) collective-permute-start(bf16[768,256]{1,0:T(8,128)(2,1)} %get-tuple-element.16.refs_4_), channel_id=1, source_target_pairs={{0,8},{4,12},{8,0},{12,4},{16,24},{20,28},{24,16},{28,20},{1,9},{5... | collective-permute-start | bytes 1179656 | tf_op jit(solution)/shard_map/ppermute | solution.py:335
  105.9 18.3 %collective-permute-start.14 = (bf16[768,256]{1,0:T(8,128)(2,1)}, bf16[768,256]{1,0:T(8,128)(2,1)}, u32[]{:S(2)}, u32[]{:S(2)}) collective-permute-start(bf16[768,256]{1,0:T(8,128)(2,1)} %get-tuple-element.16.refs_4_), channel_id=1, source_target_pairs={{0,4},{4,0},{8,12},{12,8},{16,20},{20,16},{24,28},{28,24},{1,5},{5... | collective-permute-start | bytes 1179656 | tf_op jit(solution)/shard_map/ppermute | solution.py:335
  121.9 13.1 %collective-permute-start.16 = (bf16[768,256]{1,0:T(8,128)(2,1)}, bf16[768,256]{1,0:T(8,128)(2,1)}, u32[]{:S(2)}, u32[]{:S(2)}) collective-permute-start(bf16[768,256]{1,0:T(8,128)(2,1)} %collective-permute-done.15.refs_6_), channel_id=1, source_target_pairs={{0,4},{4,0},{8,12},{12,8},{16,20},{20,16},{24,28},{28,24},{1,5},{5... | collective-permute-start | bytes 1179656 | tf_op jit(solution)/shard_map/ppermute | solution.py:335
  123.3 23.3 %collective-permute-start.10 = (bf16[768,256]{1,0:T(8,128)(2,1)}, bf16[768,256]{1,0:T(8,128)(2,1)}, u32[]{:S(2)}, u32[]{:S(2)}) collective-permute-start(bf16[768,256]{1,0:T(8,128)(2,1)} %get-tuple-element.15.refs_4_), channel_id=1, source_target_pairs={{0,4},{4,0},{8,12},{12,8},{16,20},{20,16},{24,28},{28,24},{1,5},{5... | collective-permute-start | bytes 1179656 | tf_op jit(solution)/shard_map/ppermute | solution.py:335
  123.9 29.3 %collective-permute-start.11 = (bf16[768,256]{1,0:T(8,128)(2,1)}, bf16[768,256]{1,0:T(8,128)(2,1)}, u32[]{:S(2)}, u32[]{:S(2)}) collective-permute-start(bf16[768,256]{1,0:T(8,128)(2,1)} %get-tuple-element.15.refs_4_), channel_id=1, source_target_pairs={{0,8},{4,12},{8,0},{12,4},{16,24},{20,28},{24,16},{28,20},{1,9},{5... | collective-permute-start | bytes 1179656 | tf_op jit(solution)/shard_map/ppermute | solution.py:335
  124.2 29.0 %collective-permute-start.12 = (bf16[768,256]{1,0:T(8,128)(2,1)}, bf16[768,256]{1,0:T(8,128)(2,1)}, u32[]{:S(2)}, u32[]{:S(2)}) collective-permute-start(bf16[768,256]{1,0:T(8,128)(2,1)} %get-tuple-element.15.refs_4_), channel_id=1, source_target_pairs={{0,12},{4,8},{8,4},{12,0},{16,28},{20,24},{24,20},{28,16},{1,13},{... | collective-permute-start | bytes 1179656 | tf_op jit(solution)/shard_map/ppermute | solution.py:335
  135.0 24.9 %collective-permute-start.3 = (bf16[768,128]{1,0:T(8,128)(2,1)}, bf16[768,128]{1,0:T(8,128)(2,1)S(1)}, u32[]{:S(2)}, u32[]{:S(2)}) collective-permute-start(bf16[768,128]{1,0:T(8,128)(2,1)} %get-tuple-element.22), channel_id=1, source_target_pairs={{16,0},{20,4},{24,8},{28,12},{17,1},{21,5},{25,9},{29,13},{18,2},{... | collective-permute-start | bytes 589832 | tf_op jit(solution)/shard_map/ppermute | solution.py:467
  136.3 32.2 %collective-permute-start.2 = (bf16[768,128]{1,0:T(8,128)(2,1)}, bf16[768,128]{1,0:T(8,128)(2,1)S(1)}, u32[]{:S(2)}, u32[]{:S(2)}) collective-permute-start(bf16[768,128]{1,0:T(8,128)(2,1)} %get-tuple-element.19), channel_id=1, source_target_pairs={{16,0},{20,4},{24,8},{28,12},{17,1},{21,5},{25,9},{29,13},{18,2},{... | collective-permute-start | bytes 589832 | tf_op jit(solution)/shard_map/ppermute | solution.py:467
  146.6 27.4 %collective-permute-start.17 = (bf16[512,256]{1,0:T(8,128)(2,1)}, bf16[512,256]{1,0:T(8,128)(2,1)S(1)}, u32[]{:S(2)}, u32[]{:S(2)}) collective-permute-start(bf16[512,256]{1,0:T(8,128)(2,1)} %get-tuple-element.26), channel_id=1, source_target_pairs={{0,16},{4,20},{8,24},{12,28},{16,0},{20,4},{24,8},{28,12},{1,17},{... | collective-permute-start | bytes 786440 | tf_op jit(solution)/shard_map/ppermute | solution.py:335
  159.7 18.5 %collective-permute-start.13 = (bf16[512,256]{1,0:T(8,128)(2,1)}, bf16[512,256]{1,0:T(8,128)(2,1)S(1)}, u32[]{:S(2)}, u32[]{:S(2)}) collective-permute-start(bf16[512,256]{1,0:T(8,128)(2,1)} %get-tuple-element.24), channel_id=1, source_target_pairs={{0,16},{4,20},{8,24},{12,28},{16,0},{20,4},{24,8},{28,12},{1,17},{... | collective-permute-start | bytes 786440 | tf_op jit(solution)/shard_map/ppermute | solution.py:335
  (17 other events, 163.9 us)

commit v3 on v2

--- a/solution.py
+++ b/solution.py
@@ -15,7 +15,7 @@
 ROW = 2 * DH
 
 
-def attn_kernel(chosen_ref, slot_ref, first_ref, q_ref, o_ref, lse_ref, kv_ref, dq_ref, tab_ref,
+def attn_kernel(chosen_ref, slot_ref, first_ref, q_ref, o_ref, lse_ref, kv_ref, dq_ref, dqt_ref, tab_ref,
                 x, xt, kvg, p_s, d_s, ds_s, acc, *, nsel, group, at, unroll, scale):
     i = pl.program_id(0)
     cols = group * QB
@@ -90,7 +90,9 @@
             r = pl.ds(pl.multiple_of(slots[j] * BLK, BLK), BLK)
             acc[r, :] += g[j * BLK:(j + 1) * BLK]
         stack = jnp.concatenate([dqt[:, a * QB:(a + 1) * QB] for a in range(group)], axis=0)
-        dq_ref[pl.ds(u * QB, QB), :] = (scale * stack.T).astype(dq_ref.dtype)
+        stack = scale * stack
+        dqt_ref[:, pl.ds(u * QB, QB)] = stack.astype(dqt_ref.dtype)
+        dq_ref[pl.ds(u * QB, QB), :] = stack.T.astype(dq_ref.dtype)
 
     blocks = [prepare(u) for u in range(unroll)]
     deltas = [[scores(u, h, blocks[u][1]) for h in range(cols // pair)] for u in range(unroll)]
@@ -123,6 +125,7 @@
             ],
             out_specs=[
                 pl.BlockSpec((rows, group * DH), lambda i, *_: (i, 0)),
+                pl.BlockSpec((group * DH, rows), lambda i, *_: (0, i)),
                 pl.BlockSpec(kv.shape, lambda i, *_: (0, 0)),
             ],
             scratch_shapes=[
@@ -137,6 +140,7 @@
         ),
         out_shape=[
             jax.ShapeDtypeStruct((nq * QB, group * DH), jnp.bfloat16),
+            jax.ShapeDtypeStruct((group * DH, nq * QB), jnp.bfloat16),
             jax.ShapeDtypeStruct(kv.shape, jnp.bfloat16),
         ],
         compiler_params=pltpu.CompilerParams(dimension_semantics=("arbitrary",)),
@@ -245,11 +249,12 @@
 
 def weight_kernel(place_ref, inputs_ref, *refs, near, pieces):
     sources = refs[:4 + near]
-    own_ref, other_ref, rows_t, parts, quarters, sems = refs[4 + near:]
-    tok = parts.shape[1]
+    own_ref, other_ref, rows_t, quarters, sems = refs[4 + near:]
+    tok = rows_t.shape[1] // near
     size = sources[0].shape[1]
     copies = [
-        pltpu.make_async_copy(sources[4 + k], parts.at[k], sems.at[k]) for k in range(near)
+        pltpu.make_async_copy(sources[4 + k], rows_t.at[:, pl.ds(k * tok, tok)], sems.at[k])
+        for k in range(near)
     ]
     local, rest = [], []
     for k in range(4):
@@ -266,9 +271,8 @@
         for copy in local[k * pieces:(k + 1) * pieces]:
             copy.start()
         rest[k].start()
-    for k in range(near):
-        copies[k].wait()
-        rows_t[:, pl.ds(k * tok, tok)] = parts[k].T
+    for copy in copies:
+        copy.wait()
     core, chip = place_ref[0], place_ref[1]
     for pair in range(2):
         for k in (2 * pair, 2 * pair + 1):
@@ -298,7 +302,7 @@
 def weight_parts(place, inputs, quarters, parts):
     vmem = pl.BlockSpec(memory_space=pltpu.VMEM)
     near = len(parts)
-    tok, cols = parts[0].shape
+    cols, tok = parts[0].shape
     size = quarters[0].shape[1]
     pieces = (place.shape[0] - 2) // 4
     flops = 2 * near * tok * cols * 4 * size
@@ -313,7 +317,6 @@
         ],
         scratch_shapes=[
             pltpu.VMEM((cols, near * tok), jnp.bfloat16),
-            pltpu.VMEM((near, tok, cols), jnp.bfloat16),
             pltpu.VMEM((near * tok, 4 * size), jnp.bfloat16),
             pltpu.SemaphoreType.DMA((near + 4 + 4 * pieces,)),
         ],
@@ -422,15 +425,15 @@
     dqs, returned, sums = [], [], []
     nears = []
     for g in range(kv_heads):
-        dq, tab = attn(
+        dq, dqt, tab = attn(
             flat_chosen, slots, first, queries, out_grad, lse, tables[g],
             nsel=NSEL, group=group, at=g,
         )
         dqs.append(dq)
-        nears.append([dq])
+        nears.append([dqt])
         for step in range(1, near):
-            relay = g == kv_heads - 1 and step == 3
-            nears[g].append(hop(nears[g][2], 1) if relay else hop(dq, step))
+            relay = step == 3
+            nears[g].append(hop(nears[g][2], 1) if relay else hop(dqt, step))
         back = exchange(tab.reshape(near, -1, ROW), near_groups)
         returned.append(back.reshape(kv_count * capacity * BLK, ROW))
     seen = pack(got)

time: 180 us -> 186 us (1.033)
  waiting for transfers between devices: 56.8 us -> 64.3 us
  starting transfers between devices: 56.5 us -> 53.6 us
    ppermute x2, waiting for transfers between devices: 8.54 us -> 12.8 us  [shards(): away = lax.ppermute(away, 'kv', [(j + near, j) for j in range(near)])]
    ppermute x14, waiting for transfers between devices: 37.3 us -> 40.6 us  [hop(): return lax.ppermute(x, axis, [(j, j ^ step) for j in range(n)])]
    ppermute x14, starting transfers between devices: 17.9 us -> 15 us  [hop(): return lax.ppermute(x, axis, [(j, j ^ step) for j in range(n)])]
  transfers between devices with their start and end apart: 23 -> 23, of which waited for: 10 -> 10; matrix products, arithmetic and copies ran while one was open for 5% -> 4% of each run, Pallas kernels for 27% -> 26%
where the time goes in v3:
time: 186 us; the launch traced here: 185 us
  waiting for transfers between devices  64.3 us (35%)
  starting transfers between devices  53.6 us (29%)
  Pallas kernels  51.4 us (28%)
  local copies, waits for them, and re-layouts  9.08 us (5%)
  other arithmetic  5.56 us (3%)
    ppermute x14, waiting for transfers between devices, hop(): return lax.ppermute(x, axis, [(j, j ^ step) for j in range(n)])  40.6 us
    pallas_call x2, Pallas kernels, attn(): pl.pallas_call(functools.partial(attn_kernel, nsel=nsel, group=group, at=...  26.4 us
    all_to_all x5, starting transfers between devices, exchange(): lax.all_to_all(x, 'kv', split_axis=0, concat_axis=0, tiled=True, axis_ind...  26.2 us
    ppermute x14, starting transfers between devices, hop(): return lax.ppermute(x, axis, [(j, j ^ step) for j in range(n)])  15 us
    pallas_call x2, Pallas kernels, weight_parts(): pl.pallas_call(functools.partial(weight_kernel, near=near, pieces=pieces)...  12.9 us
    ppermute x2, waiting for transfers between devices, shards(): away = lax.ppermute(away, 'kv', [(j + near, j) for j in range(near)])  12.8 us
    ppermute x2, waiting for transfers between devices, shards(): lax.ppermute(heads_kv[g], 'kv', [(j, j + near) for j in range(near)])  11 us
    ppermute x2, starting transfers between devices, shards(): lax.ppermute(heads_kv[g], 'kv', [(j, j + near) for j in range(near)])  9.79 us
  transfers between devices with their start and end apart: 23, of which 10 were waited for; matrix products, arithmetic and copies ran while one was open for 4% of the time, Pallas kernels for 26%

profile of v3, /device:TPU:0, one launch (start us, length us, event | category | flops | bytes accessed | tf_op | source)
XLA Modules:
  0.0 184.9 jit_solution(3910045785891397642)
XLA Ops:
  2.8 5.3 %all-to-all-start = ((s32[4,2,6]{2,1,0:T(2,128)}), s32[4,2,6]{2,1,0:T(2,128)S(1)}, u32[]{:S(2)}, u32[]{:S(2)}) async-start(s32[4,2,6]{2,1,0:T(2,128)} %copy.12), calls=%async_computation | async-start | bytes 8192 | tf_op jit(solution)/shard_map/all_to_all | solution.py:331
  9.2 4.5 %collective-permute-start.1 = (bf16[768,128]{1,0:T(8,128)(2,1)S(1)}, bf16[768,128]{1,0:T(8,128)(2,1)S(1)}, u32[]{:S(2)}, u32[]{:S(2)}) collective-permute-start(bf16[768,128]{1,0:T(8,128)(2,1)S(1)} %get-tuple-element.35.own_ref), channel_id=1, source_target_pairs={{0,16},{4,20},{8,24},{12,28},{1,17},{5,21},{9,25},{13,29},{2,18},{... | collective-permute-start | bytes 589832 | tf_op jit(solution)/shard_map/ppermute | solution.py:400
  14.4 3.2 %collective-permute-done.1.away_ref = bf16[768,128]{1,0:T(8,128)(2,1)S(1)} collective-permute-done((bf16[768,128]{1,0:T(8,128)(2,1)S(1)}, bf16[768,128]{1,0:T(8,128)(2,1)S(1)}, u32[]{:S(2)}, u32[]{:S(2)}) %collective-permute-start.1) | collective-permute-done | bytes 196640 | tf_op jit(solution)/shard_map/ppermute | solution.py:400
  18.3 2.6 %pick_blocks.3 = bf16[3072,128]{1,0:T(8,128)(2,1)} custom-call(s32[48]{0:T(128)} %reshape.69.ids_ref, bf16[768,128]{1,0:T(8,128)(2,1)} %copy-done.7, bf16[768,128]{1,0:T(8,128)(2,1)} %copy-done.15), custom_call_target="tpu_custom_call" | custom-call | tf_op jit(solution)/shard_map/pick_blocks/pallas_call | solution.py:174
  20.9 8.1 %all-to-all-start.2 = ((bf16[4,768,128]{2,1,0:T(8,128)(2,1)}), bf16[4,768,128]{2,1,0:T(8,128)(2,1)S(1)}, u32[]{:S(2)}, u32[]{:S(2)}) async-start(bf16[4,768,128]{2,1,0:T(8,128)(2,1)} %bitcast.21), calls=%async_computation.2 | async-start | bytes 1572864 | tf_op jit(solution)/shard_map/all_to_all | solution.py:331
  28.9 5.3 %collective-permute-start = (bf16[768,128]{1,0:T(8,128)(2,1)S(1)}, bf16[768,128]{1,0:T(8,128)(2,1)S(1)}, u32[]{:S(2)}, u32[]{:S(2)}) collective-permute-start(bf16[768,128]{1,0:T(8,128)(2,1)S(1)} %get-tuple-element.34.own_ref), channel_id=1, source_target_pairs={{0,16},{4,20},{8,24},{12,28},{1,17},{5,21},{9,25},{13,29},{2,18},{... | collective-permute-start | bytes 589832 | tf_op jit(solution)/shard_map/ppermute | solution.py:400
  34.2 7.8 %collective-permute-done.away_ref = bf16[768,128]{1,0:T(8,128)(2,1)S(1)} collective-permute-done((bf16[768,128]{1,0:T(8,128)(2,1)S(1)}, bf16[768,128]{1,0:T(8,128)(2,1)S(1)}, u32[]{:S(2)}, u32[]{:S(2)}) %collective-permute-start) | collective-permute-done | bytes 196640 | tf_op jit(solution)/shard_map/ppermute | solution.py:400
  42.7 2.6 %pick_blocks.2 = bf16[3072,128]{1,0:T(8,128)(2,1)} custom-call(s32[48]{0:T(128)} %reshape.69.ids_ref, bf16[768,128]{1,0:T(8,128)(2,1)} %copy-done.6, bf16[768,128]{1,0:T(8,128)(2,1)} %copy-done.16), custom_call_target="tpu_custom_call" | custom-call | tf_op jit(solution)/shard_map/pick_blocks/pallas_call | solution.py:174
  45.3 4.5 %all-to-all-start.1 = ((bf16[4,768,128]{2,1,0:T(8,128)(2,1)}), bf16[4,768,128]{2,1,0:T(8,128)(2,1)S(1)}, u32[]{:S(2)}, u32[]{:S(2)}) async-start(bf16[4,768,128]{2,1,0:T(8,128)(2,1)} %bitcast.19), calls=%async_computation.1 | async-start | bytes 1572864 | tf_op jit(solution)/shard_map/all_to_all | solution.py:331
  55.9 13.2 %attn_bwd.3 = (bf16[768,256]{1,0:T(8,128)(2,1)}, bf16[256,768]{1,0:T(8,128)(2,1)}, bf16[3072,128]{1,0:T(8,128)(2,1)}) custom-call(s32[96]{0:T(128)} %copy-done.17, s32[96]{0:T(128)} %add_clamp_fusion.slot_ref, s32[1]{0:T(128)} %bitcast.first_ref, bf16[768,512]{1,0:T(8,128)(2,1)} %q_ref.3, bf16[768,512]{1,0:T(8,128)(2,1)} %o_ref.3, f32[8,768]{1,0:T(8,128)} %bitcast.27, ...), custom_call_target="tpu_custom_call" | custom-call | flops 4026531840 | bytes 3145728 | tf_op jit(solution)/shard_map/attn_bwd/pallas_call | solution.py:113
  69.1 4.2 %all-to-all-start.4 = ((bf16[4,768,128]{2,1,0:T(8,128)(2,1)}), bf16[4,768,128]{2,1,0:T(8,128)(2,1)S(1)}, u32[]{:S(2)}, u32[]{:S(2)}) async-start(bf16[4,768,128]{2,1,0:T(8,128)(2,1)} %bitcast.25), calls=%async_computation.4 | async-start | bytes 1572864 | tf_op jit(solution)/shard_map/all_to_all | solution.py:331
  73.3 6.4 %collective-permute-done.6.refs_2_ = bf16[768,256]{1,0:T(8,128)(2,1)S(1)} collective-permute-done((bf16[768,256]{1,0:T(8,128)(2,1)S(1)}, bf16[768,256]{1,0:T(8,128)(2,1)S(1)}, u32[]{:S(2)}, u32[]{:S(2)}) %collective-permute-start.6) | collective-permute-done | bytes 393248 | tf_op jit(solution)/shard_map/ppermute | solution.py:338
  84.2 13.2 %attn_bwd.2 = (bf16[768,256]{1,0:T(8,128)(2,1)}, bf16[256,768]{1,0:T(8,128)(2,1)}, bf16[3072,128]{1,0:T(8,128)(2,1)}) custom-call(s32[96]{0:T(128)} %copy-done.17, s32[96]{0:T(128)} %add_clamp_fusion.slot_ref, s32[1]{0:T(128)} %bitcast.first_ref, bf16[768,512]{1,0:T(8,128)(2,1)} %q_ref.3, bf16[768,512]{1,0:T(8,128)(2,1)} %o_ref.3, f32[8,768]{1,0:T(8,128)} %bitcast.28, ...), custom_call_target="tpu_custom_call" | custom-call | flops 4026531840 | bytes 3145728 | tf_op jit(solution)/shard_map/attn_bwd/pallas_call | solution.py:113
  97.4 4.2 %all-to-all-start.3 = ((bf16[4,768,128]{2,1,0:T(8,128)(2,1)}), bf16[4,768,128]{2,1,0:T(8,128)(2,1)}, u32[]{:S(2)}, u32[]{:S(2)}) async-start(bf16[4,768,128]{2,1,0:T(8,128)(2,1)} %bitcast.24), calls=%async_computation.3 | async-start | bytes 1572864 | tf_op jit(solution)/shard_map/all_to_all | solution.py:331
  101.6 3.7 %collective-permute-done.7.refs_1_ = bf16[2304,256]{1,0:T(8,128)(2,1)S(1)} collective-permute-done((bf16[2304,256]{1,0:T(8,128)(2,1)}, bf16[2304,256]{1,0:T(8,128)(2,1)S(1)}, u32[]{:S(2)}, u32[]{:S(2)}) %collective-permute-start.7) | collective-permute-done | bytes 1179680 | tf_op jit(solution)/shard_map/ppermute | solution.py:338
  107.9 14.4 %collective-permute-done.15.refs_6_ = bf16[256,768]{1,0:T(8,128)(2,1)} collective-permute-done((bf16[256,768]{1,0:T(8,128)(2,1)}, bf16[256,768]{1,0:T(8,128)(2,1)}, u32[]{:S(2)}, u32[]{:S(2)}) %collective-permute-start.15) | collective-permute-done | bytes 393248 | tf_op jit(solution)/shard_map/ppermute | solution.py:338
  124.3 5.9 %collective-permute-done.11.refs_6_ = bf16[256,768]{1,0:T(8,128)(2,1)} collective-permute-done((bf16[256,768]{1,0:T(8,128)(2,1)}, bf16[256,768]{1,0:T(8,128)(2,1)}, u32[]{:S(2)}, u32[]{:S(2)}) %collective-permute-start.11) | collective-permute-done | bytes 393248 | tf_op jit(solution)/shard_map/ppermute | solution.py:338
  142.9 6.4 %weight_parts.3 = (f32[512,256]{1,0:T(8,128)}, bf16[512,256]{1,0:T(8,128)(2,1)}) custom-call(s32[6]{0:T(128)} %stack.27.place_ref, bf16[768,4096]{1,0:T(8,128)(2,1)} %inputs_ref.3, bf16[2304,256]{1,0:T(8,128)(2,1)} %pack.1.refs_0_, bf16[2304,256]{1,0:T(8,128)(2,1)} %copy-done, bf16[2304,256]{1,0:T(8,128)(2,1)} %copy-done.1, bf16[2304,256]{1,0:T(8,128)(2,1)} %copy-done.2, ...), custom_call_target="tpu_custom_call" | custom-call | flops 1610612736 | bytes 7077888 | tf_op jit(solution)/shard_map/weight_parts/pallas_call | solution.py:309
  149.4 3.6 %collective-permute-start.17 = (bf16[512,256]{1,0:T(8,128)(2,1)}, bf16[512,256]{1,0:T(8,128)(2,1)S(1)}, u32[]{:S(2)}, u32[]{:S(2)}) collective-permute-start(bf16[512,256]{1,0:T(8,128)(2,1)} %get-tuple-element.30), channel_id=1, source_target_pairs={{0,16},{4,20},{8,24},{12,28},{16,0},{20,4},{24,8},{28,12},{1,17},{... | collective-permute-start | bytes 786440 | tf_op jit(solution)/shard_map/ppermute | solution.py:338
  153.0 6.5 %weight_parts.2 = (f32[512,256]{1,0:T(8,128)}, bf16[512,256]{1,0:T(8,128)(2,1)}) custom-call(s32[6]{0:T(128)} %stack.27.place_ref, bf16[768,4096]{1,0:T(8,128)(2,1)} %inputs_ref.3, bf16[2304,256]{1,0:T(8,128)(2,1)} %pack.1.refs_0_, bf16[2304,256]{1,0:T(8,128)(2,1)} %copy-done, bf16[2304,256]{1,0:T(8,128)(2,1)} %copy-done.1, bf16[2304,256]{1,0:T(8,128)(2,1)} %copy-done.2, ...), custom_call_target="tpu_custom_call" | custom-call | flops 1610612736 | bytes 7077888 | tf_op jit(solution)/shard_map/weight_parts/pallas_call | solution.py:309
  159.8 8.6 %collective-permute-done.3 = bf16[768,128]{1,0:T(8,128)(2,1)S(1)} collective-permute-done((bf16[768,128]{1,0:T(8,128)(2,1)}, bf16[768,128]{1,0:T(8,128)(2,1)S(1)}, u32[]{:S(2)}, u32[]{:S(2)}) %collective-permute-start.3) | collective-permute-done | bytes 196640 | tf_op jit(solution)/shard_map/ppermute | solution.py:470
  168.4 4.2 %collective-permute-done.2 = bf16[768,128]{1,0:T(8,128)(2,1)S(1)} collective-permute-done((bf16[768,128]{1,0:T(8,128)(2,1)}, bf16[768,128]{1,0:T(8,128)(2,1)S(1)}, u32[]{:S(2)}, u32[]{:S(2)}) %collective-permute-start.2) | collective-permute-done | bytes 196640 | tf_op jit(solution)/shard_map/ppermute | solution.py:470
  173.6 4.6 %collective-permute-done.17 = bf16[512,256]{1,0:T(8,128)(2,1)S(1)} collective-permute-done((bf16[512,256]{1,0:T(8,128)(2,1)}, bf16[512,256]{1,0:T(8,128)(2,1)S(1)}, u32[]{:S(2)}, u32[]{:S(2)}) %collective-permute-start.17) | collective-permute-done | bytes 262176 | tf_op jit(solution)/shard_map/ppermute | solution.py:338
  178.3 5.5 %collective-permute-done.13 = bf16[512,256]{1,0:T(8,128)(2,1)S(1)} collective-permute-done((bf16[512,256]{1,0:T(8,128)(2,1)}, bf16[512,256]{1,0:T(8,128)(2,1)S(1)}, u32[]{:S(2)}, u32[]{:S(2)}) %collective-permute-start.13) | collective-permute-done | bytes 262176 | tf_op jit(solution)/shard_map/ppermute | solution.py:338
  (94 shorter events, 35.7 us)
Async XLA Ops:
  2.8 10.9 %all-to-all-start = ((s32[4,2,6]{2,1,0:T(2,128)}), s32[4,2,6]{2,1,0:T(2,128)S(1)}, u32[]{:S(2)}, u32[]{:S(2)}) async-start(s32[4,2,6]{2,1,0:T(2,128)} %copy.12), calls=%async_computation | async-start | bytes 8192 | tf_op jit(solution)/shard_map/all_to_all | solution.py:331
  9.2 8.4 %collective-permute-start.1 = (bf16[768,128]{1,0:T(8,128)(2,1)S(1)}, bf16[768,128]{1,0:T(8,128)(2,1)S(1)}, u32[]{:S(2)}, u32[]{:S(2)}) collective-permute-start(bf16[768,128]{1,0:T(8,128)(2,1)S(1)} %get-tuple-element.35.own_ref), channel_id=1, source_target_pairs={{0,16},{4,20},{8,24},{12,28},{1,17},{5,21},{9,25},{13,29},{2,18},{... | collective-permute-start | bytes 589832 | tf_op jit(solution)/shard_map/ppermute | solution.py:400
  20.9 24.4 %all-to-all-start.2 = ((bf16[4,768,128]{2,1,0:T(8,128)(2,1)}), bf16[4,768,128]{2,1,0:T(8,128)(2,1)S(1)}, u32[]{:S(2)}, u32[]{:S(2)}) async-start(bf16[4,768,128]{2,1,0:T(8,128)(2,1)} %bitcast.21), calls=%async_computation.2 | async-start | bytes 1572864 | tf_op jit(solution)/shard_map/all_to_all | solution.py:331
  28.9 13.1 %collective-permute-start = (bf16[768,128]{1,0:T(8,128)(2,1)S(1)}, bf16[768,128]{1,0:T(8,128)(2,1)S(1)}, u32[]{:S(2)}, u32[]{:S(2)}) collective-permute-start(bf16[768,128]{1,0:T(8,128)(2,1)S(1)} %get-tuple-element.34.own_ref), channel_id=1, source_target_pairs={{0,16},{4,20},{8,24},{12,28},{1,17},{5,21},{9,25},{13,29},{2,18},{... | collective-permute-start | bytes 589832 | tf_op jit(solution)/shard_map/ppermute | solution.py:400
  45.3 23.8 %all-to-all-start.1 = ((bf16[4,768,128]{2,1,0:T(8,128)(2,1)}), bf16[4,768,128]{2,1,0:T(8,128)(2,1)S(1)}, u32[]{:S(2)}, u32[]{:S(2)}) async-start(bf16[4,768,128]{2,1,0:T(8,128)(2,1)} %bitcast.19), calls=%async_computation.1 | async-start | bytes 1572864 | tf_op jit(solution)/shard_map/all_to_all | solution.py:331
  51.8 21.5 %collective-permute-start.4 = (bf16[768,256]{1,0:T(8,128)(2,1)}, bf16[768,256]{1,0:T(8,128)(2,1)S(1)}, u32[]{:S(2)}, u32[]{:S(2)}) collective-permute-start(bf16[768,256]{1,0:T(8,128)(2,1)} %get-tuple-element.33), channel_id=1, source_target_pairs={{0,4},{4,0},{8,12},{12,8},{16,20},{20,16},{24,28},{28,24},{1,5},{5... | collective-permute-start | bytes 1179656 | tf_op jit(solution)/shard_map/ppermute | solution.py:338
  53.8 19.5 %collective-permute-start.5 = (bf16[768,256]{1,0:T(8,128)(2,1)S(1)}, bf16[768,256]{1,0:T(8,128)(2,1)S(1)}, u32[]{:S(2)}, u32[]{:S(2)}) collective-permute-start(bf16[768,256]{1,0:T(8,128)(2,1)S(1)} %get-tuple-element.32), channel_id=1, source_target_pairs={{0,8},{4,12},{8,0},{12,4},{16,24},{20,28},{24,16},{28,20},{1,9},{5... | collective-permute-start | bytes 1179656 | tf_op jit(solution)/shard_map/ppermute | solution.py:338
  55.3 24.4 %collective-permute-start.6 = (bf16[768,256]{1,0:T(8,128)(2,1)S(1)}, bf16[768,256]{1,0:T(8,128)(2,1)S(1)}, u32[]{:S(2)}, u32[]{:S(2)}) collective-permute-start(bf16[768,256]{1,0:T(8,128)(2,1)S(1)} %get-tuple-element.31), channel_id=1, source_target_pairs={{0,12},{4,8},{8,4},{12,0},{16,28},{20,24},{24,20},{28,16},{1,13},{... | collective-permute-start | bytes 1179656 | tf_op jit(solution)/shard_map/ppermute | solution.py:338
  69.1 28.2 %all-to-all-start.4 = ((bf16[4,768,128]{2,1,0:T(8,128)(2,1)}), bf16[4,768,128]{2,1,0:T(8,128)(2,1)S(1)}, u32[]{:S(2)}, u32[]{:S(2)}) async-start(bf16[4,768,128]{2,1,0:T(8,128)(2,1)} %bitcast.25), calls=%async_computation.4 | async-start | bytes 1572864 | tf_op jit(solution)/shard_map/all_to_all | solution.py:331
  82.6 22.7 %collective-permute-start.7 = (bf16[2304,256]{1,0:T(8,128)(2,1)}, bf16[2304,256]{1,0:T(8,128)(2,1)S(1)}, u32[]{:S(2)}, u32[]{:S(2)}) collective-permute-start(bf16[2304,256]{1,0:T(8,128)(2,1)} %pack.1.refs_0_), channel_id=1, source_target_pairs={{0,2},{1,3},{2,0},{3,1},{4,6},{5,7},{6,4},{7,5},{8,10},{9,11},{10,... | collective-permute-start | bytes 3538952 | tf_op jit(solution)/shard_map/ppermute | solution.py:338
  84.2 39.6 %collective-permute-start.8 = (bf16[2304,256]{1,0:T(8,128)(2,1)}, bf16[2304,256]{1,0:T(8,128)(2,1)S(1)}, u32[]{:S(2)}, u32[]{:S(2)}) collective-permute-start(bf16[2304,256]{1,0:T(8,128)(2,1)} %pack.1.refs_0_), channel_id=1, source_target_pairs={{0,1},{1,0},{2,3},{3,2},{4,5},{5,4},{6,7},{7,6},{8,9},{9,8},{10,11... | collective-permute-start | bytes 3538952 | tf_op jit(solution)/shard_map/ppermute | solution.py:338
  97.4 39.5 %all-to-all-start.3 = ((bf16[4,768,128]{2,1,0:T(8,128)(2,1)}), bf16[4,768,128]{2,1,0:T(8,128)(2,1)}, u32[]{:S(2)}, u32[]{:S(2)}) async-start(bf16[4,768,128]{2,1,0:T(8,128)(2,1)} %bitcast.24), calls=%async_computation.3 | async-start | bytes 1572864 | tf_op jit(solution)/shard_map/all_to_all | solution.py:331
  105.3 34.0 %copy-start = (bf16[2304,256]{1,0:T(8,128)(2,1)}, bf16[2304,256]{1,0:T(8,128)(2,1)S(1)}, u32[]{:S(2)}) copy-start(bf16[2304,256]{1,0:T(8,128)(2,1)S(1)} %collective-permute-done.7.refs_1_) | copy-start | bytes 3538948
  105.3 36.6 %collective-permute-start.9 = (bf16[2304,256]{1,0:T(8,128)(2,1)S(1)}, bf16[2304,256]{1,0:T(8,128)(2,1)S(1)}, u32[]{:S(2)}, u32[]{:S(2)}) collective-permute-start(bf16[2304,256]{1,0:T(8,128)(2,1)S(1)} %collective-permute-done.7.refs_1_), channel_id=1, source_target_pairs={{0,1},{1,0},{2,3},{3,2},{4,5},{5,4},{6,7},{7,6},{8,9},{9,8},{10,11... | collective-permute-start | bytes 3538952 | tf_op jit(solution)/shard_map/ppermute | solution.py:338
  105.3 17.0 %collective-permute-start.15 = (bf16[256,768]{1,0:T(8,128)(2,1)}, bf16[256,768]{1,0:T(8,128)(2,1)}, u32[]{:S(2)}, u32[]{:S(2)}) collective-permute-start(bf16[256,768]{1,0:T(8,128)(2,1)} %get-tuple-element.28.refs_4_), channel_id=1, source_target_pairs={{0,8},{4,12},{8,0},{12,4},{16,24},{20,28},{24,16},{28,20},{1,9},{5... | collective-permute-start | bytes 1179656 | tf_op jit(solution)/shard_map/ppermute | solution.py:338
  105.9 24.4 %collective-permute-start.11 = (bf16[256,768]{1,0:T(8,128)(2,1)}, bf16[256,768]{1,0:T(8,128)(2,1)}, u32[]{:S(2)}, u32[]{:S(2)}) collective-permute-start(bf16[256,768]{1,0:T(8,128)(2,1)} %get-tuple-element.25.refs_4_), channel_id=1, source_target_pairs={{0,8},{4,12},{8,0},{12,4},{16,24},{20,28},{24,16},{28,20},{1,9},{5... | collective-permute-start | bytes 1179656 | tf_op jit(solution)/shard_map/ppermute | solution.py:338
  107.3 32.0 %collective-permute-start.14 = (bf16[256,768]{1,0:T(8,128)(2,1)}, bf16[256,768]{1,0:T(8,128)(2,1)}, u32[]{:S(2)}, u32[]{:S(2)}) collective-permute-start(bf16[256,768]{1,0:T(8,128)(2,1)} %get-tuple-element.28.refs_4_), channel_id=1, source_target_pairs={{0,4},{4,0},{8,12},{12,8},{16,20},{20,16},{24,28},{28,24},{1,5},{5... | collective-permute-start | bytes 1179656 | tf_op jit(solution)/shard_map/ppermute | solution.py:338
  122.3 18.3 %collective-permute-start.16 = (bf16[256,768]{1,0:T(8,128)(2,1)}, bf16[256,768]{1,0:T(8,128)(2,1)}, u32[]{:S(2)}, u32[]{:S(2)}) collective-permute-start(bf16[256,768]{1,0:T(8,128)(2,1)} %collective-permute-done.15.refs_6_), channel_id=1, source_target_pairs={{0,4},{4,0},{8,12},{12,8},{16,20},{20,16},{24,28},{28,24},{1,5},{5... | collective-permute-start | bytes 1179656 | tf_op jit(solution)/shard_map/ppermute | solution.py:338
  123.8 29.2 %collective-permute-start.10 = (bf16[256,768]{1,0:T(8,128)(2,1)}, bf16[256,768]{1,0:T(8,128)(2,1)}, u32[]{:S(2)}, u32[]{:S(2)}) collective-permute-start(bf16[256,768]{1,0:T(8,128)(2,1)} %get-tuple-element.25.refs_4_), channel_id=1, source_target_pairs={{0,4},{4,0},{8,12},{12,8},{16,20},{20,16},{24,28},{28,24},{1,5},{5... | collective-permute-start | bytes 1179656 | tf_op jit(solution)/shard_map/ppermute | solution.py:338
  130.3 22.7 %collective-permute-start.12 = (bf16[256,768]{1,0:T(8,128)(2,1)}, bf16[256,768]{1,0:T(8,128)(2,1)}, u32[]{:S(2)}, u32[]{:S(2)}) collective-permute-start(bf16[256,768]{1,0:T(8,128)(2,1)} %collective-permute-done.11.refs_6_), channel_id=1, source_target_pairs={{0,4},{4,0},{8,12},{12,8},{16,20},{20,16},{24,28},{28,24},{1,5},{5... | collective-permute-start | bytes 1179656 | tf_op jit(solution)/shard_map/ppermute | solution.py:338
  139.3 29.1 %collective-permute-start.3 = (bf16[768,128]{1,0:T(8,128)(2,1)}, bf16[768,128]{1,0:T(8,128)(2,1)S(1)}, u32[]{:S(2)}, u32[]{:S(2)}) collective-permute-start(bf16[768,128]{1,0:T(8,128)(2,1)} %get-tuple-element.24), channel_id=1, source_target_pairs={{16,0},{20,4},{24,8},{28,12},{17,1},{21,5},{25,9},{29,13},{18,2},{... | collective-permute-start | bytes 589832 | tf_op jit(solution)/shard_map/ppermute | solution.py:470
  140.6 32.0 %collective-permute-start.2 = (bf16[768,128]{1,0:T(8,128)(2,1)}, bf16[768,128]{1,0:T(8,128)(2,1)S(1)}, u32[]{:S(2)}, u32[]{:S(2)}) collective-permute-start(bf16[768,128]{1,0:T(8,128)(2,1)} %get-tuple-element.21), channel_id=1, source_target_pairs={{16,0},{20,4},{24,8},{28,12},{17,1},{21,5},{25,9},{29,13},{18,2},{... | collective-permute-start | bytes 589832 | tf_op jit(solution)/shard_map/ppermute | solution.py:470
  149.4 28.8 %collective-permute-start.17 = (bf16[512,256]{1,0:T(8,128)(2,1)}, bf16[512,256]{1,0:T(8,128)(2,1)S(1)}, u32[]{:S(2)}, u32[]{:S(2)}) collective-permute-start(bf16[512,256]{1,0:T(8,128)(2,1)} %get-tuple-element.30), channel_id=1, source_target_pairs={{0,16},{4,20},{8,24},{12,28},{16,0},{20,4},{24,8},{28,12},{1,17},{... | collective-permute-start | bytes 786440 | tf_op jit(solution)/shard_map/ppermute | solution.py:338
  159.5 24.3 %collective-permute-start.13 = (bf16[512,256]{1,0:T(8,128)(2,1)}, bf16[512,256]{1,0:T(8,128)(2,1)S(1)}, u32[]{:S(2)}, u32[]{:S(2)}) collective-permute-start(bf16[512,256]{1,0:T(8,128)(2,1)} %get-tuple-element.27), channel_id=1, source_target_pairs={{0,16},{4,20},{8,24},{12,28},{16,0},{20,4},{24,8},{28,12},{1,17},{... | collective-permute-start | bytes 786440 | tf_op jit(solution)/shard_map/ppermute | solution.py:338
  (17 other events, 176.8 us)
